TPU v7x, 256 devices: a whole 4x4x8 slice. The times are simulated.
256 devices in a mesh: ep: 16 (over y, x), tp: 16 (over z, core).
Axes of the slice: x: 4, y: 4, z: 8, core: 2. Of those that a mesh axis runs over, the one named last changes fastest.
Arguments:
- hidden: bfloat16 [512, 2048], P('ep'), may hold values from -6 to 6
- attn_gain: float32 [2048], replicated, may hold values from 0.1 to 1.9
- query_weight: bfloat16 [2048, 1024], P(None, 'tp'), may hold values from -0.125 to 0.125
- rotary_weight: bfloat16 [2048, 512], P(None, 'tp'), may hold values from -0.125 to 0.125
- key_up: bfloat16 [16, 64, 512], P('tp'), may hold values from -0.75 to 0.75
- cache_latent: bfloat16 [512, 4096, 512], P(('ep', 'tp'))
- cache_rotary: bfloat16 [512, 32, 4096], P(('ep', 'tp')), may hold values from -6 to 6
- lengths: int32 [512], P(('ep', 'tp')), may hold values from 1 to 4096, as said below
- value_up: bfloat16 [16, 512, 64], P('tp'), may hold values from -0.25 to 0.25
- out_weight: bfloat16 [1024, 2048], P('tp'), may hold values from -0.1875 to 0.1875
- mixed_gain: float32 [2048], replicated, may hold values from 0.1 to 1.9
- moe_gain: float32 [2048], replicated, may hold values from 0.1 to 1.9
- expert_ids: int32 [512, 2], replicated, may hold values from 0 to 15, all different within a row; in each aligned block of 32 rows (0 to 31, 32 to 63, ...) at most 8 rows name the same one
- route_logits: float32 [512, 2], replicated, may hold values from -6 to 6
- gate_weight: bfloat16 [16, 2048, 7168], P('ep', None, 'tp'), may hold values from -0.125 to 0.125
- up_weight: bfloat16 [16, 2048, 7168], P('ep', None, 'tp'), may hold values from -0.125 to 0.125
- down_weight: bfloat16 [16, 7168, 2048], P('ep', 'tp'), may hold values from -0.0625 to 0.0625
- final_gain: float32 [2048], replicated, may hold values from 0.1 to 1.9
Outputs:
- layer_out: bfloat16 [512, 2048], P(('ep', 'tp'))
Inputs may be any that keep to these rules, and one draw needn't show every extreme that they name: `lengths`: some sequence has exactly 4096 filled positions. `expert_ids`: within each aligned block of 32 rows no expert is named more than 8 times, a bound that some block reaches.
All inputs are finite; a program needn't handle non-finite values.
Results may differ from a plain program's by a relative error of at most 0.023.
The roundings to bfloat16 on the way count: a program that leaves them out, or rounds other values in their place, can miss the bound.
Values may be sent and summed in bfloat16 or wider, within the bound.
No kernel may reach another device: no remote copies, remote signals or barrier semaphores. Data moves between devices by JAX's collectives and lax.ppermute only.
A program may use at most 64 MiB of HBM per device.

v0:
```python
import jax
import jax.numpy as jnp
from jax import lax
from jax.sharding import PartitionSpec as P

EPSILON = 1e-06


def sent_together(arrays, axis, split_dim, concat_dim, along):
    both = jnp.concatenate(arrays, axis=along)
    out, at, finished = (
        lax.all_to_all(both, axis, split_axis=split_dim, concat_axis=concat_dim, tiled=True),
        0,
        [],
    )
    for a in arrays:
        finished.append(lax.slice_in_dim(out, at, at + a.shape[along], axis=along))
        at += a.shape[along]
    return tuple(finished)


def cut_along(array, dim, size):
    shape = array.shape
    tiles = array.reshape(*shape[:dim], size, shape[dim] // size, *shape[dim + 1 :])
    return jnp.moveaxis(tiles, dim, 0)


def summed_on_arrival(array, axis, dim):
    size = lax.axis_size(axis)
    tiles = lax.all_to_all(cut_along(array, dim, size), axis, 0, 0, tiled=True)
    return jnp.sum(tiles.astype(jnp.float32), axis=0)


def in_order(tiles, dim):
    tiles = jnp.moveaxis(tiles, 0, dim)
    shape = tiles.shape
    return tiles.reshape(*shape[:dim], shape[dim] * shape[dim + 1], *shape[dim + 2 :])


def copy_for_each(array, axis):
    copies = jnp.broadcast_to(array, (lax.axis_size(axis), *array.shape))
    return lax.all_to_all(copies, axis, split_axis=0, concat_axis=0, tiled=True)


def gathered_copies(array, axis, dim):
    return in_order(copy_for_each(array, axis), dim)


def norm_rows(values, gain_vector):
    values = values.astype(jnp.float32)
    factor = lax.rsqrt(jnp.mean(values * values, axis=-1, keepdims=True) + EPSILON)
    return values * factor * gain_vector


def rotate(values, position):
    half_width = values.shape[-1] // 2
    inverse = 10000.0 ** (-jnp.arange(half_width, dtype=jnp.float32) / half_width)
    angles = position.astype(jnp.float32)[:, None, None] * inverse
    cosine = jnp.cos(angles)
    sine_part = jnp.sin(angles)
    first_half = values[..., :half_width]
    second = values[..., half_width:]
    return jnp.concatenate(
        [first_half * cosine - second * sine_part, second * cosine + first_half * sine_part],
        axis=-1,
    )


def slot_tables(group_ids, group_probs, experts, capacity):
    row_count, top_count = group_ids.shape
    flat_ids = group_ids.reshape(-1)
    onehot = (flat_ids[:, None] == jnp.arange(experts, dtype=jnp.int32)[None, :]).astype(jnp.int32)
    earlier = jnp.cumsum(onehot, axis=0) - onehot
    slot_index = jnp.sum(earlier * onehot, axis=1)
    target = flat_ids * capacity + slot_index
    source = jnp.arange(row_count * top_count, dtype=jnp.int32) // top_count
    slot_rows = jnp.full((experts * capacity,), row_count, jnp.int32).at[target].set(source)
    slot_gates = (
        jnp.zeros((experts * capacity,), jnp.float32).at[target].set(group_probs.reshape(-1))
    )
    return (slot_rows, slot_gates)


def expert_rows(picked, gate_weight, up_weight, down_weight):
    gate_part = jnp.einsum("jnd,jdf->jnf", picked, gate_weight, preferred_element_type=jnp.float32)
    up_part = jnp.einsum("jnd,jdf->jnf", picked, up_weight, preferred_element_type=jnp.float32)
    act = (jax.nn.silu(gate_part) * up_part).astype(jnp.bfloat16)
    return jnp.einsum("jnf,jfd->jnd", act, down_weight, preferred_element_type=jnp.float32)


def body(
    hidden,
    attn_gain,
    query_weight,
    rotary_weight,
    key_up,
    cache_latent,
    cache_rotary,
    lengths,
    value_up,
    out_weight,
    mixed_gain,
    moe_gain,
    expert_ids,
    route_logits,
    gate_weight,
    up_weight,
    down_weight,
    final_gain,
):
    group_rows, features = hidden.shape
    local_heads, nope_width, latent_width = key_up.shape
    rotary_width = rotary_weight.shape[1] // local_heads
    own_rows = cache_latent.shape[0]
    groups = lax.axis_size("ep")
    own_start = lax.axis_index("tp") * own_rows
    normed_in = norm_rows(hidden, attn_gain).astype(jnp.bfloat16)
    query_nope = jnp.dot(normed_in, query_weight, preferred_element_type=jnp.float32).astype(
        jnp.bfloat16
    )
    query_nope = query_nope.reshape(group_rows, local_heads, nope_width)
    query_pe = jnp.dot(normed_in, rotary_weight, preferred_element_type=jnp.float32).astype(
        jnp.bfloat16
    )
    query_pe = query_pe.reshape(group_rows, local_heads, rotary_width)
    query_latent = jnp.einsum(
        "shn,hnc->shc", query_nope, key_up, preferred_element_type=jnp.float32
    ).astype(jnp.bfloat16)
    query_latent, query_pe = sent_together((query_latent, query_pe), "tp", 0, 1, 2)
    query_rot = rotate(query_pe.astype(jnp.float32), lengths - 1).astype(jnp.bfloat16)
    score_scale = (nope_width + rotary_width) ** (-0.5)
    scores = jnp.einsum(
        "bhc,bpc->bhp", query_latent, cache_latent, preferred_element_type=jnp.float32
    )
    scores = scores + jnp.einsum(
        "bhr,brp->bhp", query_rot, cache_rotary, preferred_element_type=jnp.float32
    )
    scores = scores * score_scale
    visible = (
        jnp.arange(cache_latent.shape[1], dtype=jnp.int32)[None, None, :] < lengths[:, None, None]
    )
    scores = jnp.where(visible, scores, -jnp.inf)
    highest = jnp.max(scores, axis=-1, keepdims=True)
    weights = jnp.exp(scores - highest)
    probs = (weights / jnp.sum(weights, axis=-1, keepdims=True)).astype(jnp.bfloat16)
    out_latent = jnp.einsum(
        "bhp,bpc->bhc", probs, cache_latent, preferred_element_type=jnp.float32
    ).astype(jnp.bfloat16)
    out_latent = lax.all_to_all(out_latent, "tp", split_axis=1, concat_axis=0, tiled=True)
    head_out = jnp.einsum(
        "shc,hcv->shv", out_latent, value_up, preferred_element_type=jnp.float32
    ).astype(jnp.bfloat16)
    head_terms = jnp.dot(
        head_out.reshape(group_rows, -1), out_weight, preferred_element_type=jnp.float32
    )
    attended = summed_on_arrival(head_terms.astype(jnp.bfloat16), "tp", 0).astype(jnp.bfloat16)
    own_hidden = lax.dynamic_slice_in_dim(hidden, own_start, own_rows, 0)
    mixed_rows = (own_hidden.astype(jnp.float32) + norm_rows(attended, mixed_gain)).astype(
        jnp.bfloat16
    )
    own_normed = norm_rows(mixed_rows, moe_gain).astype(jnp.bfloat16)
    normed = gathered_copies(own_normed, "tp", 0)
    local_experts = gate_weight.shape[0]
    experts_all = local_experts * groups
    top_count = expert_ids.shape[1]
    capacity = 2 * group_rows * top_count // experts_all
    gate_probs = jax.nn.softmax(route_logits, axis=-1)
    group_start = lax.axis_index("ep") * group_rows
    group_ids = lax.dynamic_slice_in_dim(expert_ids, group_start, group_rows, 0)
    group_probs = lax.dynamic_slice_in_dim(gate_probs, group_start, group_rows, 0)
    slot_rows, slot_gates = slot_tables(group_ids, group_probs, experts_all, capacity)
    padded = jnp.concatenate([normed, jnp.zeros((1, features), jnp.bfloat16)], axis=0)
    outgoing = padded[slot_rows].reshape(experts_all, capacity, features)
    arrived = lax.all_to_all(outgoing, "ep", split_axis=0, concat_axis=0, tiled=True)
    slot_count = arrived.shape[1]
    picked = arrived.reshape(groups, local_experts, slot_count, features).transpose(1, 0, 2, 3)
    picked = picked.reshape(local_experts, groups * slot_count, features)
    result = expert_rows(picked, gate_weight, up_weight, down_weight)
    result = result.reshape(local_experts, groups, slot_count, features).transpose(1, 0, 2, 3)
    result = result.reshape(groups * local_experts, slot_count, features)
    returned = lax.all_to_all(
        result.astype(jnp.bfloat16), "ep", split_axis=0, concat_axis=0, tiled=True
    ).astype(result.dtype)
    weighted = returned.reshape(experts_all * capacity, features) * slot_gates[:, None]
    combined = jnp.zeros((group_rows + 1, features), jnp.float32).at[slot_rows].add(weighted)
    routed = summed_on_arrival(combined[:group_rows].astype(jnp.bfloat16), "tp", 0)
    routed = routed.astype(jnp.bfloat16)
    return (mixed_rows.astype(jnp.float32) + norm_rows(routed, final_gain)).astype(jnp.bfloat16)


def solution(mesh):
    placed = (
        P("ep", None),
        P(),
        P(None, "tp"),
        P(None, "tp"),
        P("tp", None, None),
        P(("ep", "tp"), None, None),
        P(("ep", "tp"), None, None),
        P(("ep", "tp")),
        P("tp", None, None),
        P("tp", None),
        P(),
        P(),
        P(),
        P(),
        P("ep", None, "tp"),
        P("ep", None, "tp"),
        P("ep", "tp", None),
        P(),
    )
    return jax.shard_map(
        body, mesh=mesh, in_specs=placed, out_specs=P(("ep", "tp"), None), check_vma=False
    )
```

profile of v0, /device:TPU:1, one launch (start us, length us, event | category | flops | bytes accessed | tf_op | source)
XLA Modules:
  0.0 128.5 jit_solution(15817545877620568125)
XLA Ops:
  0.0 1.2 fusion.23
  1.2 1.2 fusion.17
  2.4 1.5 %fusion.16 = bf16[32,1,512]{2,0,1:T(8,128)(2,1)S(1)} fusion(bf16[2048,64]{0,1:T(8,128)(2,1)} %param.20, bf16[1,64,512]{2,1,0:T(8,128)(2,1)} %param.22, bf16[32,2048]{1,0:T(8,128)(2,1)} %param.18, f32[2048]{0:T(1024)} %param.19, f32[32]{0:T(128)S(1)} %add_rsqrt_fusion.3), kind=kOutput, calls=%fused_computation.21 | convolution fusion | flops 10766336 | bytes 499840 | tf_op jit(solution)/shard_map/shn,hnc->shc/dot_general | solution.py:126
  3.9 0.5 broadcast.209
  4.4 0.7 reduce.3
  5.1 0.6 reshape.283
  5.7 10.0 %all-to-all-start = ((bf16[16,2,544]{2,1,0:T(2,128)(2,1)}), bf16[16,2,544]{2,1,0:T(2,128)(2,1)S(1)}, u32[]{:S(2)}, u32[]{:S(2)}) async-start(bf16[16,2,544]{2,1,0:T(2,128)(2,1)} %reshape.283), calls=%async_computation | async-start | bytes 81920 | tf_op jit(solution)/shard_map/all_to_all | solution.py:12
  15.7 0.7 add_convert_fusion.1
  16.3 0.7 iota_compare_fusion.1
  17.1 0.8 broadcast_multiply_fusion
  18.1 0.1 multiply_cosine_fusion
  18.3 4.8 %all-to-all-done = bf16[16,2,544]{2,1,0:T(2,128)(2,1)S(1)} async-done(((bf16[16,2,544]{2,1,0:T(2,128)(2,1)}), bf16[16,2,544]{2,1,0:T(2,128)(2,1)S(1)}, u32[]{:S(2)}, u32[]{:S(2)}) %all-to-all-start) | async-done | bytes 34848 | tf_op jit(solution)/shard_map/all_to_all | solution.py:12
  23.1 0.2 reduce.2
  23.4 5.7 %fusion.35 = f32[2,16,4096]{2,1,0:T(8,128)S(1)} fusion(bf16[2,4096,512]{2,1,0:T(8,128)(2,1)} %param.23, bf16[2,16,544]{2,1,0:T(8,128)(2,1)S(1)} %bitcast.73), kind=kOutput, calls=%fused_computation.46 | convolution fusion | flops 134217728 | bytes 8945664 | tf_op jit(solution)/shard_map/bhc,bpc->bhp/dot_general | solution.py:132
  29.3 0.3 fusion.3
  29.5 0.3 fusion.60
  29.8 4.7 %convolution_convert_fusion.2 = bf16[2,16,512]{2,1,0:T(8,128)(2,1)S(1)} fusion(bf16[2,4096,512]{2,1,0:T(8,128)(2,1)} %param.23, f32[2,16]{1,0:T(2,128)S(1)} %fusion.60, f32[2,16,4096]{2,1,0:T(8,128)S(1)} %fusion.3), kind=kOutput, calls=%fused_computation.19 | convolution fusion | flops 134631456 | bytes 8945792 | tf_op jit(solution)/shard_map/bhp,bpc->bhc/dot_general | solution.py:146
  34.5 0.6 copy.52
  35.2 3.7 %all-to-all-start.1 = ((bf16[2,16,512]{2,0,1:T(2,128)(2,1)}), bf16[2,16,512]{2,0,1:T(2,128)(2,1)S(1)}, u32[]{:S(2)}, u32[]{:S(2)}) async-start(bf16[2,16,512]{2,0,1:T(2,128)(2,1)} %copy.52), calls=%async_computation.1 | async-start | bytes 65536 | tf_op jit(solution)/shard_map/all_to_all | solution.py:149
  38.9 0.2 select_reduce_fusion
  39.0 7.3 %all-to-all-done.1 = bf16[2,16,512]{2,0,1:T(2,128)(2,1)S(1)} async-done(((bf16[2,16,512]{2,0,1:T(2,128)(2,1)}), bf16[2,16,512]{2,0,1:T(2,128)(2,1)S(1)}, u32[]{:S(2)}, u32[]{:S(2)}) %all-to-all-start.1) | async-done | bytes 32800 | tf_op jit(solution)/shard_map/all_to_all | solution.py:149
  46.4 0.3 convolution_convert_fusion.1
  46.7 0.7 reshape.228
  47.5 3.7 %all-to-all-start.2 = ((bf16[16,2,2048]{2,1,0:T(2,128)(2,1)}), bf16[16,2,2048]{2,1,0:T(2,128)(2,1)S(1)}, u32[]{:S(2)}, u32[]{:S(2)}) async-start(bf16[16,2,2048]{2,1,0:T(2,128)(2,1)} %reshape.228), calls=%async_computation.2 | async-start | bytes 262144 | tf_op jit(solution)/shard_map/all_to_all | solution.py:30
  51.4 0.8 scatter_custom_fusion
  52.1 8.2 %all-to-all-done.2 = bf16[16,2,2048]{2,1,0:T(2,128)(2,1)S(1)} async-done(((bf16[16,2,2048]{2,1,0:T(2,128)(2,1)}), bf16[16,2,2048]{2,1,0:T(2,128)(2,1)S(1)}, u32[]{:S(2)}, u32[]{:S(2)}) %all-to-all-start.2) | async-done | bytes 131104 | tf_op jit(solution)/shard_map/all_to_all | solution.py:30
  60.3 0.1 reduce_sum.91
  60.5 0.1 fusion.38
  60.6 1.0 fusion.44
  61.7 0.7 broadcast_in_dim.27
  62.4 3.4 %all-to-all-start.3 = ((bf16[16,2,2048]{2,1,0:T(2,128)(2,1)}), bf16[16,2,2048]{2,1,0:T(2,128)(2,1)S(1)}, u32[]{:S(2)}, u32[]{:S(2)}) async-start(bf16[16,2,2048]{2,1,0:T(2,128)(2,1)} %broadcast_in_dim.27), calls=%async_computation.3 | async-start | bytes 262144 | tf_op jit(solution)/shard_map/all_to_all | solution.py:42
  65.8 8.4 %all-to-all-done.3 = bf16[16,2,2048]{2,1,0:T(2,128)(2,1)S(1)} async-done(((bf16[16,2,2048]{2,1,0:T(2,128)(2,1)}), bf16[16,2,2048]{2,1,0:T(2,128)(2,1)S(1)}, u32[]{:S(2)}, u32[]{:S(2)}) %all-to-all-start.3) | async-done | bytes 131104 | tf_op jit(solution)/shard_map/all_to_all | solution.py:42
  74.3 0.9 gather_fusion
  75.3 17.8 %all_to_all.58 = bf16[16,8,2048]{2,1,0:T(8,128)(2,1)S(1)} all-to-all(bf16[16,8,2048]{2,1,0:T(8,128)(2,1)S(1)} %bitcast.71), channel_id=1, replica_groups=mesh['ep'=16,'tp'=16] {'ep'}, dimensions={0} | all-to-all | bytes 1048576 | tf_op jit(solution)/shard_map/all_to_all | solution.py:174
  93.1 2.1 %fusion.8 = f32[128,448]{0,1:T(8,128)S(1)} fusion(bf16[1,2048,448]{1,2,0:T(8,128)(2,1)} %param.32, bf16[16,8,2048]{2,1,0:T(8,128)(2,1)S(1)} %all_to_all.58), kind=kOutput, calls=%fused_computation.15 | convolution fusion | flops 234881024 | bytes 2588672 | tf_op jit(solution)/shard_map/jnd,jdf->jnf/dot_general | solution.py:85
  95.2 0.6 fusion.13
  95.9 0.1 copy.55
  96.0 1.2 convolution_convert_fusion
  97.3 3.7 %all-to-all-start.5 = ((bf16[16,8,2048]{2,1,0:T(8,128)(2,1)}), bf16[16,8,2048]{2,1,0:T(8,128)(2,1)S(1)}, u32[]{:S(2)}, u32[]{:S(2)}) async-start(bf16[16,8,2048]{2,1,0:T(8,128)(2,1)} %convolution_convert_fusion), calls=%async_computation.5 | async-start | bytes 1048576 | tf_op jit(solution)/shard_map/all_to_all | solution.py:181
  101.3 0.1 reshape.261
  101.4 0.8 scatter_custom_fusion.1
  102.2 9.1 %all-to-all-done.5 = bf16[16,8,2048]{2,1,0:T(8,128)(2,1)S(1)} async-done(((bf16[16,8,2048]{2,1,0:T(8,128)(2,1)}), bf16[16,8,2048]{2,1,0:T(8,128)(2,1)S(1)}, u32[]{:S(2)}, u32[]{:S(2)}) %all-to-all-start.5) | async-done | bytes 524320 | tf_op jit(solution)/shard_map/all_to_all | solution.py:181
  111.3 2.4 %scatter_custom_fusion.2 = f32[33,2048]{1,0:T(8,128)S(1)} fusion(s32[128]{0:T(128)S(1)} %compare_select_fusion, bf16[16,8,2048]{2,1,0:T(8,128)(2,1)S(1)} %all-to-all-done.5, f32[128]{0:T(128)S(1)} %scatter_custom_fusion.1, f32[]{:T(128)} %constant.32.clone.1), kind=kCustom, calls=%fused_computation.27 | custom fusion | flops 786432 | bytes 795140 | tf_op jit(solution)/shard_map/scatter-add | solution.py:185
  113.7 0.1 reshape.238
  113.8 13.8 %all_to_all.59 = bf16[16,2,2048]{2,1,0:T(2,128)(2,1)S(1)} all-to-all(bf16[16,2,2048]{2,1,0:T(2,128)(2,1)S(1)} %reshape.238), channel_id=1, replica_groups=mesh['ep'=16,'tp'=16] {'tp'}, dimensions={0} | all-to-all | bytes 262144 | tf_op jit(solution)/shard_map/all_to_all | solution.py:30
  127.5 0.1 reduce_sum.97
  127.6 0.1 fusion.42
  127.8 0.7 fusion.47
  (49 shorter events, 1.3 us)
Async XLA Ops:
  0.0 96.0 %copy-start = (bf16[1,448,2048]{2,1,0:T(8,128)(2,1)S(1)}, bf16[1,448,2048]{2,1,0:T(8,128)(2,1)}, u32[]{:S(2)}) copy-start(bf16[1,448,2048]{2,1,0:T(8,128)(2,1)} %param.34) | copy-start | bytes 5505028
  5.7 17.4 %all-to-all-start = ((bf16[16,2,544]{2,1,0:T(2,128)(2,1)}), bf16[16,2,544]{2,1,0:T(2,128)(2,1)S(1)}, u32[]{:S(2)}, u32[]{:S(2)}) async-start(bf16[16,2,544]{2,1,0:T(2,128)(2,1)} %reshape.283), calls=%async_computation | async-start | bytes 81920 | tf_op jit(solution)/shard_map/all_to_all | solution.py:12
  23.4 5.8 %copy-start.1 = (bf16[2,32,4096]{2,1,0:T(8,128)(2,1)S(1)}, bf16[2,32,4096]{2,1,0:T(8,128)(2,1)}, u32[]{:S(2)}) copy-start(bf16[2,32,4096]{2,1,0:T(8,128)(2,1)} %param.24) | copy-start | bytes 1572868
  29.8 16.6 %copy-start.2 = (bf16[64,2048]{1,0:T(8,128)(2,1)S(1)}, bf16[64,2048]{1,0:T(8,128)(2,1)}, u32[]{:S(2)}) copy-start(bf16[64,2048]{1,0:T(8,128)(2,1)} %param.27) | copy-start | bytes 786436
  29.8 16.6 %copy-start.3 = (bf16[1,512,64]{1,2,0:T(8,128)(2,1)S(1)}, bf16[1,512,64]{1,2,0:T(8,128)(2,1)}, u32[]{:S(2)}) copy-start(bf16[1,512,64]{1,2,0:T(8,128)(2,1)} %param.26) | copy-start | bytes 196612
  29.8 30.8 %copy-start.6 = (f32[2048]{0:T(1024)S(1)}, f32[2048]{0:T(1024)}, u32[]{:S(2)}) copy-start(f32[2048]{0:T(1024)} %param.28) | copy-start | bytes 24580
  29.8 31.8 %copy-start.5 = (f32[2048]{0:T(1024)S(1)}, f32[2048]{0:T(1024)}, u32[]{:S(2)}) copy-start(f32[2048]{0:T(1024)} %param.29) | copy-start | bytes 24580
  35.2 11.2 %all-to-all-start.1 = ((bf16[2,16,512]{2,0,1:T(2,128)(2,1)}), bf16[2,16,512]{2,0,1:T(2,128)(2,1)S(1)}, u32[]{:S(2)}, u32[]{:S(2)}) async-start(bf16[2,16,512]{2,0,1:T(2,128)(2,1)} %copy.52), calls=%async_computation.1 | async-start | bytes 65536 | tf_op jit(solution)/shard_map/all_to_all | solution.py:149
  47.5 12.9 %all-to-all-start.2 = ((bf16[16,2,2048]{2,1,0:T(2,128)(2,1)}), bf16[16,2,2048]{2,1,0:T(2,128)(2,1)S(1)}, u32[]{:S(2)}, u32[]{:S(2)}) async-start(bf16[16,2,2048]{2,1,0:T(2,128)(2,1)} %reshape.228), calls=%async_computation.2 | async-start | bytes 262144 | tf_op jit(solution)/shard_map/all_to_all | solution.py:30
  62.4 11.9 %all-to-all-start.3 = ((bf16[16,2,2048]{2,1,0:T(2,128)(2,1)}), bf16[16,2,2048]{2,1,0:T(2,128)(2,1)S(1)}, u32[]{:S(2)}, u32[]{:S(2)}) async-start(bf16[16,2,2048]{2,1,0:T(2,128)(2,1)} %broadcast_in_dim.27), calls=%async_computation.3 | async-start | bytes 262144 | tf_op jit(solution)/shard_map/all_to_all | solution.py:42
  75.3 20.0 %copy-start.8 = (bf16[1,2048,448]{1,2,0:T(8,128)(2,1)S(1)}, bf16[1,2048,448]{1,2,0:T(8,128)(2,1)}, u32[]{:S(2)}) copy-start(bf16[1,2048,448]{1,2,0:T(8,128)(2,1)} %param.33) | copy-start | bytes 5505028
  95.9 5.1 %copy-start.4 = (f32[512,2]{0,1:T(2,128)S(1)}, f32[512,2]{0,1:T(2,128)}, u32[]{:S(2)}) copy-start(f32[512,2]{0,1:T(2,128)} %param.31) | copy-start | bytes 12292
  97.3 30.5 %copy-start.7 = (f32[2048]{0:T(1024)S(1)}, f32[2048]{0:T(1024)}, u32[]{:S(2)}) copy-start(f32[2048]{0:T(1024)} %param.35) | copy-start | bytes 24580
  97.3 14.0 %all-to-all-start.5 = ((bf16[16,8,2048]{2,1,0:T(8,128)(2,1)}), bf16[16,8,2048]{2,1,0:T(8,128)(2,1)S(1)}, u32[]{:S(2)}, u32[]{:S(2)}) async-start(bf16[16,8,2048]{2,1,0:T(8,128)(2,1)} %convolution_convert_fusion), calls=%async_computation.5 | async-start | bytes 1048576 | tf_op jit(solution)/shard_map/all_to_all | solution.py:181
where the time goes:
time: 129 us; the launch traced here: 128 us
  waiting for transfers between devices  37.8 us (29%)
  blocking collectives  31.6 us (24%)
  starting transfers between devices  24.5 us (19%)
  matrix products  17.7 us (14%)
  other arithmetic  9.78 us (8%)
  local copies, waits for them, and re-layouts  6.83 us (5%)
    all_to_all x1, blocking collectives, body(): lax.all_to_all(outgoing, 'ep', split_axis=0, concat_axis=0, tiled=True)  17.8 us
    all_to_all x1, blocking collectives, summed_on_arrival(): tiles = lax.all_to_all(cut_along(array, dim, size), axis, 0, 0, tiled=True)  13.8 us
    all_to_all x1, starting transfers between devices, sent_together(): lax.all_to_all(both, axis, split_axis=split_dim, concat_axis=concat_dim,...  9.97 us
    all_to_all x1, waiting for transfers between devices, body(): lax.all_to_all(result.astype(jnp.bfloat16), 'ep', split_axis=0, concat_ax...  9.09 us
    all_to_all x1, waiting for transfers between devices, copy_for_each(): return lax.all_to_all(copies, axis, split_axis=0, concat_axis=0, tiled=True)  8.42 us
    all_to_all x1, waiting for transfers between devices, summed_on_arrival(): tiles = lax.all_to_all(cut_along(array, dim, size), axis, 0, 0, tiled=True)  8.19 us
    all_to_all x1, waiting for transfers between devices, body(): lax.all_to_all(out_latent, 'tp', split_axis=1, concat_axis=0, tiled=True)  7.3 us
    dot_general x1, matrix products, body(): jnp.einsum('bhc,bpc->bhp', query_latent, cache_latent, preferred_element_...  5.72 us
  transfers between devices with their start and end apart: 5, of which 5 were waited for; matrix products, arithmetic and copies ran while one was open for 4% of the time, Pallas kernels for 0%

commit v1 on v0

v1 whole, which is shorter than its diff:
```python
import functools

import jax
import jax.numpy as jnp
from jax import lax
from jax.experimental import pallas as pl
from jax.experimental.pallas import tpu as pltpu
from jax.sharding import PartitionSpec as P

EPSILON = 1e-06
BLOCK = 1024
NEG = float("-inf")
VMEM = pl.BlockSpec(memory_space=pltpu.VMEM)
SMEM = pl.BlockSpec(memory_space=pltpu.SMEM)
ANY = pl.BlockSpec(memory_space=pl.ANY)
FULL_LIMIT = 60 * 1024 * 1024
SMALL_LIMIT = 8 * 1024 * 1024
NT = (((1,), (1,)), ((), ()))


def call(kernel, name, outs, ins, args, scratch=(), limit=SMALL_LIMIT, flops=0):
    return pl.pallas_call(
        kernel,
        out_shape=outs,
        in_specs=ins,
        out_specs=jax.tree.map(lambda _: VMEM, outs),
        scratch_shapes=list(scratch),
        compiler_params=pltpu.CompilerParams(vmem_limit_bytes=limit),
        cost_estimate=pl.CostEstimate(flops=flops, bytes_accessed=0, transcendentals=0),
        name=name,
    )(*args)


def shape(dims, dtype):
    return jax.ShapeDtypeStruct(dims, dtype)


def norm_rows(values, gain_vector):
    values = values.astype(jnp.float32)
    factor = lax.rsqrt(jnp.mean(values * values, axis=-1, keepdims=True) + EPSILON)
    return values * factor * gain_vector


def rotate(values, position):
    half_width = values.shape[-1] // 2
    inverse = 10000.0 ** (-jnp.arange(half_width, dtype=jnp.float32) / half_width)
    angles = position.astype(jnp.float32)[:, None, None] * inverse
    cosine = jnp.cos(angles)
    sine_part = jnp.sin(angles)
    first_half = values[..., :half_width]
    second = values[..., half_width:]
    return jnp.concatenate(
        [first_half * cosine - second * sine_part, second * cosine + first_half * sine_part],
        axis=-1,
    )


def query_kernel(hidden_ref, gain_ref, query_ref, rotary_ref, key_ref, out_ref):
    latent = key_ref.shape[1]
    normed = norm_rows(hidden_ref[...], gain_ref[...]).astype(jnp.bfloat16)
    nope = lax.dot_general(
        normed, query_ref[...], NT, preferred_element_type=jnp.float32
    ).astype(jnp.bfloat16)
    turned = lax.dot_general(normed, rotary_ref[...], NT, preferred_element_type=jnp.float32)
    out_ref[:, :latent] = jnp.dot(
        nope, key_ref[...], preferred_element_type=jnp.float32
    ).astype(jnp.bfloat16)
    out_ref[:, latent:] = turned.astype(jnp.bfloat16)


def queries(hidden, gain, query_weight, rotary_weight, key_up):
    rows = hidden.shape[0]
    width = key_up.shape[1] + rotary_weight.shape[1]
    return call(
        query_kernel,
        "queries",
        shape((rows, width), jnp.bfloat16),
        [VMEM] * 5,
        (hidden, gain[None, :], query_weight.T, rotary_weight.T, key_up),
    )


def attend_kernel(
    scale, lengths_ref, query_ref, rot_ref, latent_hbm, rotary_hbm, out_ref,
    latent_ref, rotary_ref, s_ref, latent_sems, rotary_sems,
):
    rows, heads, width = query_ref.shape
    most = latent_hbm.shape[1] // BLOCK

    def copies(s, b):
        at = pl.ds(b * BLOCK, BLOCK)
        return (
            pltpu.make_async_copy(
                latent_hbm.at[s, at, :], latent_ref.at[s, at, :], latent_sems.at[s, b]
            ),
            pltpu.make_async_copy(
                rotary_hbm.at[s, :, at], rotary_ref.at[s, :, at], rotary_sems.at[s, b]
            ),
        )

    counts = [lax.div(lengths_ref[s] + (BLOCK - 1), BLOCK) for s in range(rows)]
    for s in range(rows):
        for b in range(most):

            @pl.when(b < counts[s])
            def _start(s=s, b=b):
                for copy in copies(s, b):
                    copy.start()

    for s in range(rows):
        length = lengths_ref[s]
        blocks = counts[s]
        latent_query = query_ref[s]
        rotary_query = rot_ref[s]

        def score_block(b, highest):
            at = pl.multiple_of(b * BLOCK, BLOCK)
            for copy in copies(s, b):
                copy.wait()
            part = lax.dot_general(
                latent_query, latent_ref[s, pl.ds(at, BLOCK), :], NT,
                preferred_element_type=jnp.float32,
            )
            part = part + jnp.dot(
                rotary_query, rotary_ref[s, :, pl.ds(at, BLOCK)], preferred_element_type=jnp.float32
            )
            places = at + lax.broadcasted_iota(jnp.int32, (heads, BLOCK), 1)
            part = jnp.where(places < length, part * scale, NEG)
            s_ref[:, pl.ds(at, BLOCK)] = part
            return jnp.maximum(highest, jnp.max(part, axis=1, keepdims=True))

        highest = lax.fori_loop(0, blocks, score_block, jnp.full((heads, 1), NEG, jnp.float32))

        def weigh_block(b, total):
            at = pl.multiple_of(b * BLOCK, BLOCK)
            weights = jnp.exp(s_ref[:, pl.ds(at, BLOCK)] - highest)
            s_ref[:, pl.ds(at, BLOCK)] = weights
            return total + jnp.sum(weights, axis=1, keepdims=True)

        total = lax.fori_loop(0, blocks, weigh_block, jnp.zeros((heads, 1), jnp.float32))

        def sum_block(b, summed):
            at = pl.multiple_of(b * BLOCK, BLOCK)
            probs = (s_ref[:, pl.ds(at, BLOCK)] / total).astype(jnp.bfloat16)
            return summed + jnp.dot(
                probs, latent_ref[s, pl.ds(at, BLOCK), :], preferred_element_type=jnp.float32
            )

        summed = lax.fori_loop(0, blocks, sum_block, jnp.zeros((heads, width), jnp.float32))
        out_ref[s] = summed.astype(jnp.bfloat16)


def attend(query, rot, latent, rotary, lengths, scale):
    rows, heads, width = query.shape
    blocks = latent.shape[1] // BLOCK
    return call(
        functools.partial(attend_kernel, scale),
        "attend",
        shape((rows, heads, width), jnp.bfloat16),
        [SMEM, VMEM, VMEM, ANY, ANY],
        (lengths, query, rot, latent, rotary),
        scratch=(
            pltpu.VMEM(latent.shape, latent.dtype),
            pltpu.VMEM(rotary.shape, rotary.dtype),
            pltpu.VMEM((heads, latent.shape[1]), jnp.float32),
            pltpu.SemaphoreType.DMA((rows, blocks)),
            pltpu.SemaphoreType.DMA((rows, blocks)),
        ),
        limit=FULL_LIMIT,
        flops=4 * latent.size * heads,
    )


def mix_kernel(terms_ref, own_ref, mixed_gain_ref, moe_gain_ref, mixed_ref, send_ref):
    peers, rows, half = send_ref.shape
    attended = terms_ref[0].astype(jnp.float32)
    for t in range(1, peers):
        attended = attended + terms_ref[t].astype(jnp.float32)
    attended = attended.astype(jnp.bfloat16)
    mixed = (
        own_ref[...].astype(jnp.float32) + norm_rows(attended, mixed_gain_ref[...])
    ).astype(jnp.bfloat16)
    mixed_ref[...] = mixed
    normed = norm_rows(mixed, moe_gain_ref[...]).astype(jnp.bfloat16)
    for t in range(peers):
        send_ref[t] = normed[:, (t % 2) * half : (t % 2 + 1) * half]


def mix(terms, own, mixed_gain, moe_gain):
    peers, rows, features = terms.shape
    return call(
        mix_kernel,
        "mix",
        (
            shape((rows, features), jnp.bfloat16),
            shape((peers, rows, features // 2), jnp.bfloat16),
        ),
        [VMEM] * 4,
        (terms, own, mixed_gain[None, :], moe_gain[None, :]),
    )


def dispatch_kernel(target_ref, rows_ref, out_ref):
    slots, rows = out_ref.shape[0], rows_ref.shape[0]
    place = lax.broadcasted_iota(jnp.int32, (slots, rows), 0)
    taken = (place == target_ref[0:1, :]) | (place == target_ref[1:2, :])
    pick = jnp.where(taken, 1.0, 0.0).astype(jnp.bfloat16)
    out_ref[...] = jnp.dot(pick, rows_ref[...], preferred_element_type=jnp.float32).astype(
        jnp.bfloat16
    )


def dispatch(target, rows, slots):
    return call(
        dispatch_kernel,
        "dispatch",
        shape((slots, rows.shape[1]), jnp.bfloat16),
        [VMEM] * 2,
        (target, rows),
    )


def combine_kernel(target_ref, gates_ref, returned_ref, out_ref):
    rows, slots = out_ref.shape[0], returned_ref.shape[0]
    place = lax.broadcasted_iota(jnp.int32, (rows, slots), 1)
    gates = jnp.where(place == target_ref[:, 0:1], gates_ref[:, 0:1], 0.0)
    gates = gates + jnp.where(place == target_ref[:, 1:2], gates_ref[:, 1:2], 0.0)
    returned = returned_ref[...]
    total = None
    for _ in range(3):
        part = gates.astype(jnp.bfloat16)
        term = jnp.dot(part, returned, preferred_element_type=jnp.float32)
        total = term if total is None else total + term
        gates = gates - part.astype(jnp.float32)
    out_ref[...] = total.astype(jnp.bfloat16)


def combine(target, gates, returned):
    return call(
        combine_kernel,
        "combine",
        shape((target.shape[0], returned.shape[1]), jnp.bfloat16),
        [VMEM] * 3,
        (target, gates, returned),
    )


def finish_kernel(terms_ref, mixed_ref, gain_ref, out_ref):
    peers = terms_ref.shape[0]
    halves = []
    for c in range(2):
        part = terms_ref[c].astype(jnp.float32)
        for t in range(c + 2, peers, 2):
            part = part + terms_ref[t].astype(jnp.float32)
        halves.append(part)
    routed = jnp.concatenate(halves, axis=1).astype(jnp.bfloat16)
    out_ref[...] = (
        mixed_ref[...].astype(jnp.float32) + norm_rows(routed, gain_ref[...])
    ).astype(jnp.bfloat16)


def finish(terms, mixed, gain):
    return call(
        finish_kernel,
        "finish",
        shape(mixed.shape, jnp.bfloat16),
        [VMEM] * 3,
        (terms, mixed, gain[None, :]),
    )


def enter_kernel(core_ref, rows_ref, gate_ref, up_ref, gate_out, up_out):
    half = rows_ref.shape[1]
    at = pl.ds(pl.multiple_of(core_ref[0] * half, half), half)
    rows = rows_ref[...]
    gate_out[...] = lax.dot_general(rows, gate_ref[:, at], NT, preferred_element_type=jnp.float32)
    up_out[...] = lax.dot_general(rows, up_ref[:, at], NT, preferred_element_type=jnp.float32)


def leave_kernel(core_ref, rows_ref, gate_ref, up_ref, down_ref, gate_part, up_part, act_ref, out_ref):
    half = rows_ref.shape[1]
    at = pl.ds(pl.multiple_of((1 - core_ref[0]) * half, half), half)
    rows = rows_ref[...]
    gate = gate_part[...] + lax.dot_general(
        rows, gate_ref[:, at], NT, preferred_element_type=jnp.float32
    )
    up = up_part[...] + lax.dot_general(
        rows, up_ref[:, at], NT, preferred_element_type=jnp.float32
    )
    act = (gate / (1.0 + jnp.exp(-gate)) * up).astype(jnp.bfloat16)
    act_ref[...] = act
    out_ref[...] = jnp.dot(act, down_ref[:, at], preferred_element_type=jnp.float32).astype(
        jnp.bfloat16
    )


def close_kernel(core_ref, act_ref, down_ref, out_ref):
    half = out_ref.shape[1]
    at = pl.ds(pl.multiple_of(core_ref[0] * half, half), half)
    out_ref[...] = jnp.dot(act_ref[...], down_ref[:, at], preferred_element_type=jnp.float32)


def expert_rows(rows, gate_weight, up_weight, down_weight, core, pairs):
    slots, half = rows.shape
    width = gate_weight.shape[0]
    other = lax.ppermute(rows, "tp", pairs)
    gate_part, up_part = call(
        enter_kernel,
        "enter",
        (shape((slots, width), jnp.float32), shape((slots, width), jnp.float32)),
        [SMEM] + [VMEM] * 3,
        (core, rows, gate_weight, up_weight),
        flops=4 * slots * half * width,
    )
    act, sent = call(
        leave_kernel,
        "leave",
        (shape((slots, width), jnp.bfloat16), shape((slots, half), jnp.bfloat16)),
        [SMEM] + [VMEM] * 6,
        (core, other, gate_weight, up_weight, down_weight, gate_part, up_part),
        flops=6 * slots * half * width,
    )
    arrived = lax.ppermute(sent, "tp", pairs)
    kept = call(
        close_kernel,
        "close",
        shape((slots, half), jnp.float32),
        [SMEM] + [VMEM] * 2,
        (core, act, down_weight),
        flops=2 * slots * half * width,
    )
    return (kept + arrived.astype(jnp.float32)).astype(jnp.bfloat16)


def slot_targets(group_ids, experts, capacity):
    row_count, top_count = group_ids.shape
    flat_ids = group_ids.reshape(-1)
    onehot = (flat_ids[:, None] == jnp.arange(experts, dtype=jnp.int32)[None, :]).astype(jnp.int32)
    earlier = jnp.cumsum(onehot, axis=0) - onehot
    slot_index = jnp.sum(earlier * onehot, axis=1)
    return (flat_ids * capacity + slot_index).reshape(row_count, top_count)


def exchanged(array, axis):
    return lax.all_to_all(array, axis, split_axis=0, concat_axis=0, tiled=True)


def body(
    hidden,
    attn_gain,
    query_weight,
    rotary_weight,
    key_up,
    cache_latent,
    cache_rotary,
    lengths,
    value_up,
    out_weight,
    mixed_gain,
    moe_gain,
    expert_ids,
    route_logits,
    gate_weight,
    up_weight,
    down_weight,
    final_gain,
):
    group_rows, features = hidden.shape
    _, nope_width, latent_width = key_up.shape
    rotary_width = rotary_weight.shape[1]
    own_rows = cache_latent.shape[0]
    groups = lax.axis_size("ep")
    peers = lax.axis_size("tp")
    place = lax.axis_index("tp")
    core = (place % 2).astype(jnp.int32).reshape(1)
    pairs = [(i, i ^ 1) for i in range(peers)]
    half = features // 2
    top_count = expert_ids.shape[1]
    capacity = 2 * group_rows * top_count // groups

    query = queries(hidden, attn_gain, query_weight, rotary_weight, key_up[0])
    query = exchanged(query.reshape(peers, own_rows, -1), "tp")

    gate_probs = jax.nn.softmax(route_logits, axis=-1)
    group_start = lax.axis_index("ep") * group_rows
    group_ids = lax.dynamic_slice_in_dim(expert_ids, group_start, group_rows, 0)
    group_gates = lax.dynamic_slice_in_dim(gate_probs, group_start, group_rows, 0)
    target = slot_targets(group_ids, groups, capacity)
    own_hidden = lax.dynamic_slice_in_dim(hidden, place * own_rows, own_rows, 0)

    query = query.transpose(1, 0, 2)
    query_latent = query[:, :, :latent_width]
    query_pe = query[:, :, latent_width:]
    query_rot = rotate(query_pe.astype(jnp.float32), lengths - 1).astype(jnp.bfloat16)
    score_scale = (nope_width + rotary_width) ** (-0.5)
    query_latent, query_rot, target, group_gates, own_hidden = lax.optimization_barrier(
        (query_latent, query_rot, target, group_gates, own_hidden)
    )
    out_latent = attend(query_latent, query_rot, cache_latent, cache_rotary, lengths, score_scale)
    out_latent = exchanged(out_latent.transpose(1, 0, 2), "tp")
    head_out = jnp.dot(
        out_latent.reshape(group_rows, latent_width), value_up[0], preferred_element_type=jnp.float32
    ).astype(jnp.bfloat16)
    head_terms = jnp.dot(head_out, out_weight, preferred_element_type=jnp.float32)
    head_terms = head_terms.astype(jnp.bfloat16).reshape(peers, own_rows, features)
    head_terms = exchanged(head_terms, "tp")
    mixed_rows, normed = mix(head_terms, own_hidden, mixed_gain, moe_gain)
    normed = exchanged(normed, "tp").reshape(group_rows, half)
    outgoing = dispatch(target.T, normed, groups * capacity)
    arrived = exchanged(outgoing.reshape(groups, capacity, half), "ep")
    result = expert_rows(
        arrived.reshape(groups * capacity, half),
        gate_weight[0].T,
        up_weight[0].T,
        down_weight[0],
        core,
        pairs,
    )
    returned = exchanged(result.reshape(groups, capacity, half), "ep")
    combined = combine(target, group_gates, returned.reshape(groups * capacity, half))
    terms = exchanged(combined.reshape(peers, own_rows, half), "tp")
    return finish(terms, mixed_rows, final_gain)


def solution(mesh):
    placed = (
        P("ep", None),
        P(),
        P(None, "tp"),
        P(None, "tp"),
        P("tp", None, None),
        P(("ep", "tp"), None, None),
        P(("ep", "tp"), None, None),
        P(("ep", "tp")),
        P("tp", None, None),
        P("tp", None),
        P(),
        P(),
        P(),
        P(),
        P("ep", None, "tp"),
        P("ep", None, "tp"),
        P("ep", "tp", None),
        P(),
    )
    return jax.shard_map(
        body, mesh=mesh, in_specs=placed, out_specs=P(("ep", "tp"), None), check_vma=False
    )
```

time: 129 us -> 114 us (0.88)
  blocking collectives: 31.6 us -> 61.3 us
  waiting for transfers between devices: 37.8 us -> 11.1 us
  matrix products: 17.7 us -> 0.32 us
  Pallas kernels: 0 us -> 11.5 us
  starting transfers between devices: 24.5 us -> 14.9 us
  other arithmetic: 9.78 us -> 3.44 us
  local copies, waits for them, and re-layouts: 6.83 us -> 11.1 us
    all_to_all x2 -> x5, blocking collectives: 31.6 us -> 61.3 us  [exchanged(): return lax.all_to_all(array, axis, split_axis=0, concat_axis=0, tiled=True)]
    all_to_all x5 -> x2, waiting for transfers between devices: 37.8 us -> 9.91 us  [exchanged(): return lax.all_to_all(array, axis, split_axis=0, concat_axis=0, tiled=True)]
    dot_general x9 -> x1, matrix products: 17.7 us -> 0.32 us  [body(): jnp.dot(head_out, out_weight, preferred_element_type=jnp.float32)]
    pallas_call x0 -> x9, Pallas kernels: none -> 11.5 us  [call(): pl.pallas_call(kernel, out_shape=outs, in_specs=ins, out_specs=jax.tree.m...]
    all_to_all x5 -> x2, starting transfers between devices: 24.5 us -> 13.4 us  [exchanged(): return lax.all_to_all(array, axis, split_axis=0, concat_axis=0, tiled=True)]
    unnamed x20 -> x27, local copies, waits for them, and re-layouts: 0.73 us -> 6.76 us
    reduce_sum x7 -> x1, other arithmetic: 2.81 us -> 0.18 us  [slot_targets(): slot_index = jnp.sum(earlier * onehot, axis=1)]
    scatter-add x1 -> x0, other arithmetic: 2.35 us -> none  [body(): jnp.zeros((group_rows + 1, features), jnp.float32).at[slot_rows]]
  transfers between devices with their start and end apart: 5 -> 4, of which waited for: 5 -> 3; matrix products, arithmetic and copies ran while one was open for 4% -> 4% of each run, Pallas kernels for 0% -> 1%
where the time goes in v1:
time: 114 us
  blocking collectives  61.3 us (54%)
  starting transfers between devices  14.9 us (13%)
  Pallas kernels  11.5 us (10%)
  local copies, waits for them, and re-layouts  11.1 us (10%)
  waiting for transfers between devices  11.1 us (10%)
  other arithmetic  3.44 us (3%)
    all_to_all x5, blocking collectives, exchanged(): return lax.all_to_all(array, axis, split_axis=0, concat_axis=0, tiled=True)  61.3 us
    all_to_all x2, starting transfers between devices, exchanged(): return lax.all_to_all(array, axis, split_axis=0, concat_axis=0, tiled=True)  13.4 us
    pallas_call x9, Pallas kernels, call(): pl.pallas_call(kernel, out_shape=outs, in_specs=ins, out_specs=jax.tree.m...  11.5 us
    all_to_all x2, waiting for transfers between devices, exchanged(): return lax.all_to_all(array, axis, split_axis=0, concat_axis=0, tiled=True)  9.91 us
    unnamed x27, local copies, waits for them, and re-layouts  6.76 us
  transfers between devices with their start and end apart: 4, of which 3 were waited for; matrix products, arithmetic and copies ran while one was open for 4% of the time, Pallas kernels for 1%

profile of v1, /device:TPU:1, one launch (start us, length us, event | category | flops | bytes accessed | tf_op | source)
XLA Modules:
  0.0 113.8 jit_solution(9668432927214795223)
XLA Ops:
  0.0 1.0 copy-done.4
  1.0 0.9 copy-done.5
  1.9 0.9 copy-done.6
  2.8 0.8 copy-done.7
  3.6 0.7 copy-done.8
  4.3 0.5 queries.1
  4.8 0.6 reshape.96
  5.4 10.0 %all-to-all-start = ((bf16[16,2,544]{2,1,0:T(2,128)(2,1)}), bf16[16,2,544]{2,1,0:T(2,128)(2,1)S(1)}, u32[]{:S(2)}, u32[]{:S(2)}) async-start(bf16[16,2,544]{2,1,0:T(2,128)(2,1)} %reshape.96), calls=%async_computation | async-start | bytes 81920 | tf_op jit(solution)/shard_map/all_to_all | solution.py:345
  15.4 0.7 add_convert_fusion.2
  16.1 0.7 reduce_max.9
  16.8 0.7 fusion.4
  17.5 0.8 constant_dynamic-slice_fusion.1
  18.3 0.8 constant_dynamic-slice_fusion.own_ref
  19.1 0.1 copy.48
  19.2 0.1 eq.17
  19.4 0.1 reduce_window_sum.11
  19.5 0.2 select_reduce_fusion
  19.7 0.1 reduce_sum.21
  19.8 0.1 multiply_cosine_fusion
  19.9 0.1 dynamic-slice_divide_fusion
  20.0 0.1 copy.49.gates_ref
  20.1 2.8 %all-to-all-done = bf16[16,2,544]{2,1,0:T(2,128)(2,1)S(1)} async-done(((bf16[16,2,544]{2,1,0:T(2,128)(2,1)}), bf16[16,2,544]{2,1,0:T(2,128)(2,1)S(1)}, u32[]{:S(2)}, u32[]{:S(2)}) %all-to-all-start) | async-done | bytes 34848 | tf_op jit(solution)/shard_map/all_to_all | solution.py:345
  22.9 0.6 slice.16.query_ref
  23.5 0.7 pad_maximum_fusion.rot_ref
  24.2 7.0 %attend.1 = bf16[2,16,512]{2,1,0:T(8,128)(2,1)} custom-call(s32[2]{0:T(128)} %lengths_ref.1, bf16[2,16,512]{2,1,0:T(8,128)(2,1)} %slice.16.query_ref, bf16[2,16,32]{2,1,0:T(8,128)(2,1)} %pad_maximum_fusion.rot_ref, bf16[2,4096,512]{2,1,0:T(8,128)(2,1)} %latent_hbm.1, bf16[2,32,4096]{2,1,0:T(8,128)(2,1)} %rotary_hbm.1), custom_call_target="tpu_custom_call" | custom-call | flops 268435456 | tf_op jit(solution)/shard_map/attend/pallas_call | solution.py:22
  31.3 0.9 copy.45
  32.2 11.6 %all_to_all.35 = bf16[16,2,512]{2,1,0:T(2,128)(2,1)S(1)} all-to-all(bf16[16,2,512]{2,1,0:T(2,128)(2,1)S(1)} %copy.45), channel_id=1, replica_groups=mesh['ep'=16,'tp'=16] {'tp'}, dimensions={0} | all-to-all | bytes 65536 | tf_op jit(solution)/shard_map/all_to_all | solution.py:345
  43.8 0.3 convolution_convert_fusion
  44.2 0.1 reshape.99
  44.3 12.0 %all_to_all.36.terms_ref = bf16[16,2,2048]{2,1,0:T(2,128)(2,1)S(1)} all-to-all(bf16[16,2,2048]{2,1,0:T(2,128)(2,1)S(1)} %reshape.99), channel_id=1, replica_groups=mesh['ep'=16,'tp'=16] {'tp'}, dimensions={0} | all-to-all | bytes 262144 | tf_op jit(solution)/shard_map/all_to_all | solution.py:345
  56.3 0.9 mix.1
  57.1 3.4 %all-to-all-start.3 = ((bf16[16,2,1024]{2,1,0:T(2,128)(2,1)}), bf16[16,2,1024]{2,1,0:T(2,128)(2,1)S(1)}, u32[]{:S(2)}, u32[]{:S(2)}) async-start(bf16[16,2,1024]{2,1,0:T(2,128)(2,1)} %get-tuple-element.21), calls=%async_computation.3 | async-start | bytes 131072 | tf_op jit(solution)/shard_map/all_to_all | solution.py:345
  60.5 0.1 copy.46.target_ref
  60.6 7.2 %all-to-all-done.3 = bf16[16,2,1024]{2,1,0:T(2,128)(2,1)S(1)} async-done(((bf16[16,2,1024]{2,1,0:T(2,128)(2,1)}), bf16[16,2,1024]{2,1,0:T(2,128)(2,1)S(1)}, u32[]{:S(2)}, u32[]{:S(2)}) %all-to-all-start.3) | async-done | bytes 65568 | tf_op jit(solution)/shard_map/all_to_all | solution.py:345
  67.8 0.2 dispatch.1
  68.0 15.2 %all_to_all.37 = bf16[16,8,1024]{2,1,0:T(8,128)(2,1)S(1)} all-to-all(bf16[16,8,1024]{2,1,0:T(8,128)(2,1)S(1)} %bitcast.39), channel_id=1, replica_groups=mesh['ep'=16,'tp'=16] {'ep'}, dimensions={0} | all-to-all | bytes 524288 | tf_op jit(solution)/shard_map/all_to_all | solution.py:345
  83.2 1.4 %collective-permute-start = (bf16[128,1024]{1,0:T(8,128)(2,1)S(1)}, bf16[128,1024]{1,0:T(8,128)(2,1)S(1)}, u32[]{:S(2)}, u32[]{:S(2)}) collective-permute-start(bf16[128,1024]{1,0:T(8,128)(2,1)S(1)} %bitcast.37), channel_id=1, source_target_pairs={{0,1},{1,0},{2,3},{3,2},{4,5},{5,4},{6,7},{7,6},{8,9},{9,8},{10,11... | collective-permute-start | bytes 786440 | tf_op jit(solution)/shard_map/ppermute | solution.py:306
  84.6 1.5 %copy-done.2 = bf16[1,2048,448]{1,2,0:T(8,128)(2,1)S(1)} copy-done((bf16[1,2048,448]{1,2,0:T(8,128)(2,1)S(1)}, bf16[1,2048,448]{1,2,0:T(8,128)(2,1)}, u32[]{:S(2)}) %copy-start.2) | copy-done | bytes 1835032
  86.1 0.7 enter.1
  86.8 0.8 copy-done.3
  87.6 0.9 leave.1
  88.6 0.1 collective-permute-start.1
  88.7 0.3 close.1
  89.0 1.2 %collective-permute-done.1 = bf16[128,1024]{1,0:T(8,128)(2,1)S(1)} collective-permute-done((bf16[128,1024]{1,0:T(8,128)(2,1)S(1)}, bf16[128,1024]{1,0:T(8,128)(2,1)S(1)}, u32[]{:S(2)}, u32[]{:S(2)}) %collective-permute-start.1) | collective-permute-done | bytes 262176 | tf_op jit(solution)/shard_map/ppermute | solution.py:323
  90.3 11.0 %all_to_all.38 = bf16[16,8,1024]{2,1,0:T(8,128)(2,1)S(1)} all-to-all(bf16[16,8,1024]{2,1,0:T(8,128)(2,1)S(1)} %fusion), channel_id=1, replica_groups=mesh['ep'=16,'tp'=16] {'ep'}, dimensions={0} | all-to-all | bytes 524288 | tf_op jit(solution)/shard_map/all_to_all | solution.py:345
  101.2 0.3 combine.1
  101.6 11.5 %all_to_all.39.terms_ref = bf16[16,2,1024]{2,1,0:T(2,128)(2,1)S(1)} all-to-all(bf16[16,2,1024]{2,1,0:T(2,128)(2,1)S(1)} %reshape.105), channel_id=1, replica_groups=mesh['ep'=16,'tp'=16] {'tp'}, dimensions={0} | all-to-all | bytes 131072 | tf_op jit(solution)/shard_map/all_to_all | solution.py:345
  113.1 0.7 finish.1
  (31 shorter events, 0.4 us)
Async XLA Ops:
  0.0 43.8 %copy-start = (bf16[64,2048]{1,0:T(8,128)(2,1)S(1)}, bf16[64,2048]{1,0:T(8,128)(2,1)}, u32[]{:S(2)}) copy-start(bf16[64,2048]{1,0:T(8,128)(2,1)} %param.27) | copy-start | bytes 786436
  0.0 1.0 copy-start.4
  1.0 0.9 copy-start.5
  1.9 0.9 copy-start.6
  2.8 0.8 copy-start.7
  3.6 0.7 copy-start.8
  5.4 17.4 %all-to-all-start = ((bf16[16,2,544]{2,1,0:T(2,128)(2,1)}), bf16[16,2,544]{2,1,0:T(2,128)(2,1)S(1)}, u32[]{:S(2)}, u32[]{:S(2)}) async-start(bf16[16,2,544]{2,1,0:T(2,128)(2,1)} %reshape.96), calls=%async_computation | async-start | bytes 81920 | tf_op jit(solution)/shard_map/all_to_all | solution.py:345
  24.2 19.6 %copy-start.12 = (bf16[1,512,64]{1,2,0:T(8,128)(2,1)S(1)}, bf16[1,512,64]{1,2,0:T(8,128)(2,1)}, u32[]{:S(2)}) copy-start(bf16[1,512,64]{1,2,0:T(8,128)(2,1)} %param.26) | copy-start | bytes 196612
  24.2 32.0 %copy-start.9 = (f32[2048]{0:T(1024)S(1)}, f32[2048]{0:T(1024)}, u32[]{:S(2)}) copy-start(f32[2048]{0:T(1024)} %param.28) | copy-start | bytes 24580
  24.2 32.0 %copy-start.10 = (f32[2048]{0:T(1024)S(1)}, f32[2048]{0:T(1024)}, u32[]{:S(2)}) copy-start(f32[2048]{0:T(1024)} %param.29) | copy-start | bytes 24580
  31.3 53.4 %copy-start.1 = (bf16[1,2048,448]{1,2,0:T(8,128)(2,1)S(1)}, bf16[1,2048,448]{1,2,0:T(8,128)(2,1)}, u32[]{:S(2)}) copy-start(bf16[1,2048,448]{1,2,0:T(8,128)(2,1)} %param.32) | copy-start | bytes 5505028
  57.1 10.6 %all-to-all-start.3 = ((bf16[16,2,1024]{2,1,0:T(2,128)(2,1)}), bf16[16,2,1024]{2,1,0:T(2,128)(2,1)S(1)}, u32[]{:S(2)}, u32[]{:S(2)}) async-start(bf16[16,2,1024]{2,1,0:T(2,128)(2,1)} %get-tuple-element.21), calls=%async_computation.3 | async-start | bytes 131072 | tf_op jit(solution)/shard_map/all_to_all | solution.py:345
  83.2 3.6 %collective-permute-start = (bf16[128,1024]{1,0:T(8,128)(2,1)S(1)}, bf16[128,1024]{1,0:T(8,128)(2,1)S(1)}, u32[]{:S(2)}, u32[]{:S(2)}) collective-permute-start(bf16[128,1024]{1,0:T(8,128)(2,1)S(1)} %bitcast.37), channel_id=1, source_target_pairs={{0,1},{1,0},{2,3},{3,2},{4,5},{5,4},{6,7},{7,6},{8,9},{9,8},{10,11... | collective-permute-start | bytes 786440 | tf_op jit(solution)/shard_map/ppermute | solution.py:306
  84.6 1.5 %copy-start.2 = (bf16[1,2048,448]{1,2,0:T(8,128)(2,1)S(1)}, bf16[1,2048,448]{1,2,0:T(8,128)(2,1)}, u32[]{:S(2)}) copy-start(bf16[1,2048,448]{1,2,0:T(8,128)(2,1)} %param.33) | copy-start | bytes 5505028
  86.1 1.5 %copy-start.3 = (bf16[1,448,2048]{2,1,0:T(8,128)(2,1)S(1)}, bf16[1,448,2048]{2,1,0:T(8,128)(2,1)}, u32[]{:S(2)}) copy-start(bf16[1,448,2048]{2,1,0:T(8,128)(2,1)} %param.34) | copy-start | bytes 5505028
  88.6 1.6 %collective-permute-start.1 = (bf16[128,1024]{1,0:T(8,128)(2,1)S(1)}, bf16[128,1024]{1,0:T(8,128)(2,1)S(1)}, u32[]{:S(2)}, u32[]{:S(2)}) collective-permute-start(bf16[128,1024]{1,0:T(8,128)(2,1)S(1)} %get-tuple-element.25), channel_id=1, source_target_pairs={{0,1},{1,0},{2,3},{3,2},{4,5},{5,4},{6,7},{7,6},{8,9},{9,8},{10,11... | collective-permute-start | bytes 786440 | tf_op jit(solution)/shard_map/ppermute | solution.py:323
  88.7 24.4 %copy-start.11 = (f32[2048]{0:T(1024)S(1)}, f32[2048]{0:T(1024)}, u32[]{:S(2)}) copy-start(f32[2048]{0:T(1024)} %param.35) | copy-start | bytes 24580

commit v2 on v1

v2 whole, which is shorter than its diff:
```python
import functools

import jax
import jax.numpy as jnp
import numpy as np
from jax import lax
from jax.experimental import pallas as pl
from jax.experimental.pallas import tpu as pltpu
from jax.sharding import PartitionSpec as P

EPSILON = 1e-06
BLOCK = 1024
NEG = float("-inf")
VMEM = pl.BlockSpec(memory_space=pltpu.VMEM)
SMEM = pl.BlockSpec(memory_space=pltpu.SMEM)
HBM = pl.BlockSpec(memory_space=pltpu.HBM)
ATTEND_LIMIT = 14 * 1024 * 1024
SMALL_LIMIT = 8 * 1024 * 1024
NT = (((1,), (1,)), ((), ()))


def call(kernel, name, outs, ins, args, scratch=(), limit=SMALL_LIMIT, flops=0):
    return pl.pallas_call(
        kernel,
        out_shape=outs,
        in_specs=ins,
        out_specs=jax.tree.map(lambda _: VMEM, outs),
        scratch_shapes=list(scratch),
        compiler_params=pltpu.CompilerParams(vmem_limit_bytes=limit),
        cost_estimate=pl.CostEstimate(flops=flops, bytes_accessed=0, transcendentals=0),
        name=name,
    )(*args)


def shape(dims, dtype):
    return jax.ShapeDtypeStruct(dims, dtype)


def norm_rows(values, gain_vector):
    values = values.astype(jnp.float32)
    factor = lax.rsqrt(jnp.mean(values * values, axis=-1, keepdims=True) + EPSILON)
    return values * factor * gain_vector


def column(row):
    size = row.shape[1]
    same = lax.broadcasted_iota(jnp.int32, (size, size), 0) == lax.broadcasted_iota(
        jnp.int32, (size, size), 1
    )
    return jnp.sum(jnp.where(same, row, 0.0), axis=1, keepdims=True)


def front_kernel(
    capacity, hidden_hbm, gain_hbm, query_hbm, rotary_hbm, key_hbm, ids_hbm, logits_hbm, lengths_hbm,
    out_ref, own_ref, slots_ref, columns_ref, trig_ref,
    hidden_ref, gain_ref, query_ref, rotary_ref, key_ref, ids_ref, logits_ref, lengths_ref, sems,
):
    group_rows, features = hidden_ref.shape
    peers, own_rows, _ = out_ref.shape
    latent = key_ref.shape[1]
    pairs = (
        (lengths_hbm, lengths_ref),
        (ids_hbm, ids_ref),
        (logits_hbm, logits_ref),
        (hidden_hbm, hidden_ref),
        (gain_hbm, gain_ref),
        (query_hbm, query_ref),
        (rotary_hbm, rotary_ref),
        (key_hbm, key_ref),
    )
    copies = [pltpu.make_async_copy(s, d, sems.at[i]) for i, (s, d) in enumerate(pairs)]
    for copy in copies:
        copy.start()
    group, place = lax.axis_index("ep"), lax.axis_index("tp")

    copies[1].wait()
    copies[2].wait()
    ids_all = ids_ref[...].astype(jnp.float32)
    logits_all = logits_ref[...]
    ids = jnp.zeros((2, group_rows), jnp.float32)
    logits = jnp.zeros((2, group_rows), jnp.float32)
    for g in range(ids_all.shape[1] // group_rows):
        at = slice(g * group_rows, (g + 1) * group_rows)
        ids = jnp.where(group == g, ids_all[:, at], ids)
        logits = jnp.where(group == g, logits_all[:, at], logits)
    id_rows = [ids[k : k + 1, :] for k in range(2)]
    id_columns = [column(row) for row in id_rows]
    before = lax.broadcasted_iota(jnp.int32, (group_rows, group_rows), 0) < lax.broadcasted_iota(
        jnp.int32, (group_rows, group_rows), 1
    )
    top = jnp.maximum(logits[0:1, :], logits[1:2, :])
    weights = [jnp.exp(logits[k : k + 1, :] - top) for k in range(2)]
    for k in range(2):
        hits = jnp.where(before & (id_columns[0] == id_rows[k]), 1.0, 0.0)
        hits = hits + jnp.where(before & (id_columns[1] == id_rows[k]), 1.0, 0.0)
        slot = id_rows[k] * capacity + jnp.sum(hits, axis=0, keepdims=True)
        slots_ref[k : k + 1, :] = slot
        columns_ref[:, k : k + 1] = column(slot)
        columns_ref[:, 2 + k : 3 + k] = column(weights[k] / (weights[0] + weights[1]))

    copies[0].wait()
    half = trig_ref.shape[1] // 2
    lane = lax.broadcasted_iota(jnp.int32, (1, 2 * half), 1)
    inverse = jnp.zeros((1, 2 * half), jnp.float32)
    for i in range(half):
        value = float(np.float32(10000.0 ** (-i / half)))
        inverse = jnp.where((lane == i) | (lane == i + half), value, inverse)
    for s in range(own_rows):
        angles = (lengths_ref[s] - 1).astype(jnp.float32) * inverse
        turned = jnp.sin(angles)
        trig_ref[2 * s : 2 * s + 1, :] = jnp.cos(angles)
        trig_ref[2 * s + 1 : 2 * s + 2, :] = jnp.where(lane < half, -turned, turned)

    copies[3].wait()
    copies[4].wait()
    hidden = hidden_ref[...]
    normed = norm_rows(hidden, gain_ref[...]).astype(jnp.bfloat16)
    pick_row = lax.broadcasted_iota(jnp.int32, (8, group_rows), 0) + place * own_rows
    pick = jnp.where(pick_row == lax.broadcasted_iota(jnp.int32, (8, group_rows), 1), 1.0, 0.0)
    own = jnp.dot(pick.astype(jnp.bfloat16), hidden, preferred_element_type=jnp.float32)
    own_ref[...] = own[:own_rows].astype(jnp.bfloat16)
    copies[5].wait()
    copies[6].wait()
    copies[7].wait()
    nope = lax.dot_general(
        normed, query_ref[...], NT, preferred_element_type=jnp.float32
    ).astype(jnp.bfloat16)
    turned = lax.dot_general(normed, rotary_ref[...], NT, preferred_element_type=jnp.float32)
    projected = jnp.dot(nope, key_ref[...], preferred_element_type=jnp.float32)
    for t in range(peers):
        at = slice(t * own_rows, (t + 1) * own_rows)
        out_ref[t, :, :latent] = projected[at].astype(jnp.bfloat16)
        out_ref[t, :, latent:] = turned[at].astype(jnp.bfloat16)


def in_hbm(*arrays):
    return tuple(pltpu.with_memory_space_constraint(a, pltpu.HBM) for a in arrays)


def front(hidden, gain, query_weight, rotary_weight, key_up, ids, logits, lengths, peers, capacity):
    rows, features = hidden.shape
    own_rows = rows // peers
    rope, latent = rotary_weight.shape[1], key_up.shape[1]
    arrays = in_hbm(
        hidden, gain[None, :], query_weight.T, rotary_weight.T, key_up, ids.T, logits.T, lengths
    )
    held = [pltpu.VMEM(a.shape, a.dtype) for a in arrays[:-1]]
    return call(
        functools.partial(front_kernel, capacity),
        "front",
        (
            shape((peers, own_rows, latent + rope), jnp.bfloat16),
            shape((own_rows, features), jnp.bfloat16),
            shape((2, rows), jnp.float32),
            shape((rows, 4), jnp.float32),
            shape((2 * own_rows, rope), jnp.float32),
        ),
        [HBM] * 8,
        arrays,
        scratch=held + [pltpu.SMEM(lengths.shape, lengths.dtype), pltpu.SemaphoreType.DMA((8,))],
    )


def attend_kernel(
    scale, lengths_hbm, query_ref, trig_ref, latent_hbm, rotary_hbm, out_ref,
    lengths_ref, latent_ref, rotary_ref, latent_query, rotary_query, summed_ref,
    lengths_sem, latent_sems, rotary_sems,
):
    heads, rows, _ = query_ref.shape
    width, rope = latent_query.shape[2], rotary_query.shape[2]
    most = latent_hbm.shape[1] // BLOCK

    def copies(s, b):
        at = pl.ds(b * BLOCK, BLOCK)
        return (
            pltpu.make_async_copy(
                latent_hbm.at[s, at, :], latent_ref.at[s, at, :], latent_sems.at[s, b]
            ),
            pltpu.make_async_copy(
                rotary_hbm.at[s, :, at], rotary_ref.at[s, :, at], rotary_sems.at[s, b]
            ),
        )

    fetch = pltpu.make_async_copy(lengths_hbm, lengths_ref, lengths_sem)
    fetch.start()
    for s in range(rows):
        for copy in copies(s, 0):
            copy.start()
    swap = lax.broadcasted_iota(jnp.int32, (rope, rope), 0) == lax.rem(
        lax.broadcasted_iota(jnp.int32, (rope, rope), 1) + rope // 2, rope
    )
    swap = jnp.where(swap, 1.0, 0.0).astype(jnp.bfloat16)
    query = query_ref[...].astype(jnp.float32)
    for s in range(rows):
        own = jnp.concatenate([query[h, s : s + 1, :] for h in range(heads)], axis=0)
        latent_query[s] = own[:, :width].astype(jnp.bfloat16)
        plain = own[:, width:]
        turned = jnp.dot(plain.astype(jnp.bfloat16), swap, preferred_element_type=jnp.float32)
        rotary_query[s] = (
            plain * trig_ref[2 * s : 2 * s + 1, :] + turned * trig_ref[2 * s + 1 : 2 * s + 2, :]
        ).astype(jnp.bfloat16)
    fetch.wait()
    for s in range(rows):
        blocks = lax.div(lengths_ref[s] + (BLOCK - 1), BLOCK)
        for b in range(1, most):

            @pl.when(b < blocks)
            def _start(s=s, b=b):
                for copy in copies(s, b):
                    copy.start()

    @pl.loop(0, rows)
    def _sequence(s):
        length = lengths_ref[s]
        blocks = lax.div(length + (BLOCK - 1), BLOCK)
        for count in range(1, most + 1):

            @pl.when(blocks == count)
            def _attend(count=count):
                scores = []
                for b in range(count):
                    at = slice(b * BLOCK, (b + 1) * BLOCK)
                    for copy in copies(s, b):
                        copy.wait()
                    part = lax.dot_general(
                        latent_query[s], latent_ref[s, at, :], NT,
                        preferred_element_type=jnp.float32,
                    )
                    part = part + jnp.dot(
                        rotary_query[s], rotary_ref[s, :, at], preferred_element_type=jnp.float32
                    )
                    part = part * scale
                    if b == count - 1:
                        places = b * BLOCK + lax.broadcasted_iota(jnp.int32, (heads, BLOCK), 1)
                        part = jnp.where(places < length, part, NEG)
                    scores.append(part)
                highest = scores[0]
                for part in scores[1:]:
                    highest = jnp.maximum(highest, part)
                highest = jnp.max(highest, axis=1, keepdims=True)
                weights = [jnp.exp(part - highest) for part in scores]
                total = weights[0]
                for part in weights[1:]:
                    total = total + part
                factor = 1.0 / jnp.sum(total, axis=1, keepdims=True)
                summed = None
                for b in range(count):
                    probs = (weights[b] * factor).astype(jnp.bfloat16)
                    term = jnp.dot(
                        probs, latent_ref[s, b * BLOCK : (b + 1) * BLOCK, :],
                        preferred_element_type=jnp.float32,
                    )
                    summed = term if summed is None else summed + term
                summed_ref[s] = summed

    sums = [summed_ref[s] for s in range(rows)]
    for h in range(heads):
        out_ref[h] = jnp.concatenate([part[h : h + 1, :] for part in sums], axis=0).astype(
            jnp.bfloat16
        )


def attend(query, trig, latent, rotary, lengths, scale):
    heads, rows, _ = query.shape
    width, rope = latent.shape[2], rotary.shape[1]
    blocks = latent.shape[1] // BLOCK
    lengths, latent, rotary = in_hbm(lengths, latent, rotary)
    return call(
        functools.partial(attend_kernel, scale),
        "attend",
        shape((heads, rows, width), jnp.bfloat16),
        [HBM, VMEM, VMEM, HBM, HBM],
        (lengths, query, trig, latent, rotary),
        scratch=(
            pltpu.SMEM(lengths.shape, lengths.dtype),
            pltpu.VMEM(latent.shape, latent.dtype),
            pltpu.VMEM(rotary.shape, rotary.dtype),
            pltpu.VMEM((rows, heads, width), jnp.bfloat16),
            pltpu.VMEM((rows, heads, rope), jnp.bfloat16),
            pltpu.VMEM((rows, heads, width), jnp.float32),
            pltpu.SemaphoreType.DMA,
            pltpu.SemaphoreType.DMA((rows, blocks)),
            pltpu.SemaphoreType.DMA((rows, blocks)),
        ),
        limit=ATTEND_LIMIT,
        flops=4 * latent.size * heads,
    )


def row_sums(terms, rows, keep):
    place = lax.broadcasted_iota(jnp.int32, (8, terms.shape[0]), 1)
    wanted = (lax.rem(place, rows) == lax.broadcasted_iota(jnp.int32, place.shape, 0)) & keep(place)
    ones = jnp.where(wanted, 1.0, 0.0).astype(jnp.bfloat16)
    return jnp.dot(ones, terms, preferred_element_type=jnp.float32)


def mix_kernel(terms_ref, own_ref, mixed_gain_ref, moe_gain_ref, mixed_ref, send_ref):
    peers, rows, half = send_ref.shape
    attended = row_sums(terms_ref[...], rows, lambda place: place >= 0)[:rows].astype(jnp.bfloat16)
    mixed = (
        own_ref[...].astype(jnp.float32) + norm_rows(attended, mixed_gain_ref[...])
    ).astype(jnp.bfloat16)
    mixed_ref[...] = mixed
    normed = norm_rows(mixed, moe_gain_ref[...]).astype(jnp.bfloat16)
    for t in range(peers):
        send_ref[t] = normed[:, (t % 2) * half : (t % 2 + 1) * half]


def mix(terms, own, mixed_gain, moe_gain, peers):
    rows, features = own.shape
    return call(
        mix_kernel,
        "mix",
        (
            shape((rows, features), jnp.bfloat16),
            shape((peers, rows, features // 2), jnp.bfloat16),
        ),
        [VMEM] * 4,
        (terms, own, mixed_gain[None, :], moe_gain[None, :]),
    )


def dispatch_kernel(slots_ref, rows_ref, out_ref):
    slots, rows = out_ref.shape[0], rows_ref.shape[0]
    place = lax.broadcasted_iota(jnp.int32, (slots, rows), 0).astype(jnp.float32)
    taken = (place == slots_ref[0:1, :]) | (place == slots_ref[1:2, :])
    pick = jnp.where(taken, 1.0, 0.0).astype(jnp.bfloat16)
    out_ref[...] = jnp.dot(pick, rows_ref[...], preferred_element_type=jnp.float32).astype(
        jnp.bfloat16
    )


def dispatch(own_slots, rows, slots):
    return call(
        dispatch_kernel,
        "dispatch",
        shape((slots, rows.shape[1]), jnp.bfloat16),
        [VMEM] * 2,
        (own_slots, rows),
    )


def combine_kernel(columns_ref, returned_ref, out_ref):
    rows, slots = out_ref.shape[0], returned_ref.shape[0]
    place = lax.broadcasted_iota(jnp.int32, (rows, slots), 1).astype(jnp.float32)
    gates = jnp.where(place == columns_ref[:, 0:1], columns_ref[:, 2:3], 0.0)
    gates = gates + jnp.where(place == columns_ref[:, 1:2], columns_ref[:, 3:4], 0.0)
    returned = returned_ref[...]
    total = None
    for _ in range(3):
        part = gates.astype(jnp.bfloat16)
        term = jnp.dot(part, returned, preferred_element_type=jnp.float32)
        total = term if total is None else total + term
        gates = gates - part.astype(jnp.float32)
    out_ref[...] = total.astype(jnp.bfloat16)


def combine(columns, returned):
    return call(
        combine_kernel,
        "combine",
        shape((columns.shape[0], returned.shape[1]), jnp.bfloat16),
        [VMEM] * 2,
        (columns, returned),
    )


def finish_kernel(terms_ref, mixed_ref, gain_ref, out_ref):
    rows = mixed_ref.shape[0]
    terms = terms_ref[...]
    halves = [
        row_sums(terms, rows, lambda place, c=c: lax.rem(lax.div(place, rows), 2) == c)
        for c in range(2)
    ]
    routed = jnp.concatenate(halves, axis=1)[:rows].astype(jnp.bfloat16)
    out_ref[...] = (
        mixed_ref[...].astype(jnp.float32) + norm_rows(routed, gain_ref[...])
    ).astype(jnp.bfloat16)


def finish(terms, mixed, gain):
    return call(
        finish_kernel,
        "finish",
        shape(mixed.shape, jnp.bfloat16),
        [VMEM] * 3,
        (terms, mixed, gain[None, :]),
    )


def half_at(own, half):
    core = lax.rem(lax.axis_index("tp"), 2)
    if not own:
        core = 1 - core
    return pl.ds(pl.multiple_of(core * half, half), half)


def product(rows, weight):
    return lax.dot_general(rows, weight, NT, preferred_element_type=jnp.float32)


def enter_kernel(rows_ref, gate_ref, up_hbm, gate_out, up_out, up_ref, sem):
    half = rows_ref.shape[1]
    at = half_at(True, half)
    copy = pltpu.make_async_copy(up_hbm.at[:, at], up_ref, sem)
    copy.start()
    rows = rows_ref[...]
    gate_out[...] = product(rows, gate_ref[:, at])
    copy.wait()
    up_out[...] = product(rows, up_ref[...])


def leave_kernel(
    rows_ref, gate_ref, up_hbm, down_hbm, gate_part, up_part, act_ref, out_ref, up_ref, down_ref, sems
):
    half = rows_ref.shape[1]
    at = half_at(False, half)
    copies = [
        pltpu.make_async_copy(up_hbm.at[:, at], up_ref, sems.at[0]),
        pltpu.make_async_copy(down_hbm.at[:, at], down_ref, sems.at[1]),
    ]
    for copy in copies:
        copy.start()
    rows = rows_ref[...]
    gate = gate_part[...] + product(rows, gate_ref[:, at])
    copies[0].wait()
    up = up_part[...] + product(rows, up_ref[...])
    act = (gate / (1.0 + jnp.exp(-gate)) * up).astype(jnp.bfloat16)
    act_ref[...] = act
    copies[1].wait()
    out_ref[...] = jnp.dot(act, down_ref[...], preferred_element_type=jnp.float32).astype(
        jnp.bfloat16
    )


def close_kernel(act_ref, down_hbm, out_ref, down_ref, sem):
    copy = pltpu.make_async_copy(down_hbm.at[:, half_at(True, out_ref.shape[1])], down_ref, sem)
    copy.start()
    copy.wait()
    out_ref[...] = jnp.dot(act_ref[...], down_ref[...], preferred_element_type=jnp.float32)


def expert_rows(rows, gate_weight, up_weight, down_weight, pairs):
    slots, half = rows.shape
    width = gate_weight.shape[0]
    up_weight, down_weight = in_hbm(up_weight, down_weight)
    part = shape((slots, width), jnp.float32)
    side = pltpu.VMEM((width, half), jnp.bfloat16)
    other = lax.ppermute(rows, "tp", pairs)
    gate_part, up_part = call(
        enter_kernel,
        "enter",
        (part, part),
        [VMEM, VMEM, HBM],
        (rows, gate_weight, up_weight),
        scratch=(side, pltpu.SemaphoreType.DMA),
        flops=4 * slots * half * width,
    )
    act, sent = call(
        leave_kernel,
        "leave",
        (shape((slots, width), jnp.bfloat16), shape((slots, half), jnp.bfloat16)),
        [VMEM, VMEM, HBM, HBM, VMEM, VMEM],
        (other, gate_weight, up_weight, down_weight, gate_part, up_part),
        scratch=(side, side, pltpu.SemaphoreType.DMA((2,))),
        flops=6 * slots * half * width,
    )
    arrived = lax.ppermute(sent, "tp", pairs)
    kept = call(
        close_kernel,
        "close",
        shape((slots, half), jnp.float32),
        [VMEM, HBM],
        (act, down_weight),
        scratch=(side, pltpu.SemaphoreType.DMA),
        flops=2 * slots * half * width,
    )
    return (kept + arrived.astype(jnp.float32)).astype(jnp.bfloat16)


def exchanged(array, axis):
    return lax.all_to_all(array, axis, split_axis=0, concat_axis=0, tiled=True)


def body(
    hidden,
    attn_gain,
    query_weight,
    rotary_weight,
    key_up,
    cache_latent,
    cache_rotary,
    lengths,
    value_up,
    out_weight,
    mixed_gain,
    moe_gain,
    expert_ids,
    route_logits,
    gate_weight,
    up_weight,
    down_weight,
    final_gain,
):
    group_rows, features = hidden.shape
    _, nope_width, latent_width = key_up.shape
    rotary_width = rotary_weight.shape[1]
    own_rows = cache_latent.shape[0]
    groups = lax.axis_size("ep")
    peers = lax.axis_size("tp")
    pairs = [(i, i ^ 1) for i in range(peers)]
    half = features // 2
    capacity = 2 * group_rows * expert_ids.shape[1] // groups
    slots = groups * capacity

    query, own_hidden, own_slots, columns, trig = front(
        hidden,
        attn_gain,
        query_weight,
        rotary_weight,
        key_up[0],
        expert_ids,
        route_logits,
        lengths,
        peers,
        capacity,
    )
    query = exchanged(query, "tp")
    score_scale = (nope_width + rotary_width) ** (-0.5)
    out_latent = attend(query, trig, cache_latent, cache_rotary, lengths, score_scale)
    out_latent = exchanged(out_latent, "tp").reshape(group_rows, latent_width)
    head_out = jnp.dot(out_latent, value_up[0], preferred_element_type=jnp.float32)
    head_terms = jnp.dot(
        head_out.astype(jnp.bfloat16), out_weight, preferred_element_type=jnp.float32
    )
    head_terms = head_terms.astype(jnp.bfloat16).reshape(peers, own_rows, features)
    head_terms = exchanged(head_terms, "tp").reshape(group_rows, features)
    mixed_rows, normed = mix(head_terms, own_hidden, mixed_gain, moe_gain, peers)
    normed = exchanged(normed, "tp").reshape(group_rows, half)
    outgoing = dispatch(own_slots, normed, slots).reshape(groups, capacity, half)
    arrived = exchanged(outgoing, "ep").reshape(slots, half)
    result = expert_rows(arrived, gate_weight[0].T, up_weight[0].T, down_weight[0], pairs)
    returned = exchanged(result.reshape(groups, capacity, half), "ep").reshape(slots, half)
    combined = combine(columns, returned).reshape(peers, own_rows, half)
    terms = exchanged(combined, "tp").reshape(group_rows, half)
    return finish(terms, mixed_rows, final_gain)


def solution(mesh):
    placed = (
        P("ep", None),
        P(),
        P(None, "tp"),
        P(None, "tp"),
        P("tp", None, None),
        P(("ep", "tp"), None, None),
        P(("ep", "tp"), None, None),
        P(("ep", "tp")),
        P("tp", None, None),
        P("tp", None),
        P(),
        P(),
        P(),
        P(),
        P("ep", None, "tp"),
        P("ep", None, "tp"),
        P("ep", "tp", None),
        P(),
    )
    return jax.shard_map(
        body, mesh=mesh, in_specs=placed, out_specs=P(("ep", "tp"), None), check_vma=False
    )
```

time: 114 us -> 104 us (0.912)
  blocking collectives: 61.3 us -> 87.8 us
  starting transfers between devices: 14.9 us -> 1.36 us
  waiting for transfers between devices: 11.1 us -> 0.01 us
  local copies, waits for them, and re-layouts: 11.1 us -> 0.29 us
  other arithmetic: 3.44 us -> 0.07 us
  Pallas kernels: 11.5 us -> 13.1 us
    all_to_all x5 -> x7, blocking collectives: 61.3 us -> 87.8 us  [exchanged(): return lax.all_to_all(array, axis, split_axis=0, concat_axis=0, tiled=True)]
    all_to_all x2 -> x0, starting transfers between devices: 13.4 us -> none  [exchanged(): return lax.all_to_all(array, axis, split_axis=0, concat_axis=0, tiled=True)]
    all_to_all x2 -> x0, waiting for transfers between devices: 9.91 us -> none  [exchanged(): return lax.all_to_all(array, axis, split_axis=0, concat_axis=0, tiled=True)]
    unnamed x27 -> x12, local copies, waits for them, and re-layouts: 6.76 us -> 0.03 us
    pallas_call x9, Pallas kernels: 11.5 us -> 13.1 us  [call(): pl.pallas_call(kernel, out_shape=outs, in_specs=ins, out_specs=jax.tree.m...]
    dynamic_slice x3 -> x0, local copies, waits for them, and re-layouts: 1.6 us -> none  [the longest x1 0.77 us: body(): own_hidden = lax.dynamic_slice_in_dim(hidden, place * own_rows, own_rows, 0)]
    ppermute x1, waiting for transfers between devices: 1.2 us -> 0.01 us  [expert_rows(): arrived = lax.ppermute(sent, 'tp', pairs)]
  transfers between devices with their start and end apart: 4 -> 2, of which waited for: 3 -> 0; matrix products, arithmetic and copies ran while one was open for 4% -> 0% of each run, Pallas kernels for 1% -> 3%
where the time goes in v2:
time: 104 us; the launch traced here: 103 us
  blocking collectives  87.8 us (84%)
  Pallas kernels  13.1 us (13%)
  starting transfers between devices  1.36 us (1%)
    all_to_all x7, blocking collectives, exchanged(): return lax.all_to_all(array, axis, split_axis=0, concat_axis=0, tiled=True)  87.8 us
    pallas_call x9, Pallas kernels, call(): pl.pallas_call(kernel, out_shape=outs, in_specs=ins, out_specs=jax.tree.m...  13.1 us
  transfers between devices with their start and end apart: 2, of which 0 were waited for; matrix products, arithmetic and copies ran while one was open for 0% of the time, Pallas kernels for 3%

profile of v2, /device:TPU:1, one launch (start us, length us, event | category | flops | bytes accessed | tf_op | source)
XLA Modules:
  0.0 103.1 jit_solution(10591022840409747276)
XLA Ops:
  0.0 0.0 copy-start
  0.0 1.9 %front.1 = (bf16[16,2,544]{2,1,0:T(2,128)(2,1)S(1)}, bf16[2,2048]{1,0:T(2,128)(2,1)S(1)}, f32[2,32]{1,0:T(2,128)S(1)}, f32[32,4]{1,0:T(8,128)S(1)}, f32[4,32]{1,0:T(4,128)S(1)}) custom-call(bf16[32,2048]{1,0:T(8,128)(2,1)} %hidden_hbm.1, f32[1,2048]{1,0:T(1,128)} %bitcast.43, bf16[64,2048]{1,0:T(8,128)(2,1)} %bitcast.40, bf16[32,2048]{1,0:T(8,128)(2,1)} %bitcast.41, ...), custom_call_target="tpu_custom_call" | custom-call | tf_op jit(solution)/shard_map/front/pallas_call | solution.py:23
  1.9 17.2 %all_to_all.35.query_ref = bf16[16,2,544]{2,1,0:T(2,128)(2,1)S(1)} all-to-all(bf16[16,2,544]{2,1,0:T(2,128)(2,1)S(1)} %get-tuple-element.18), channel_id=1, replica_groups=mesh['ep'=16,'tp'=16] {'tp'}, dimensions={0} | all-to-all | bytes 69632 | tf_op jit(solution)/shard_map/all_to_all | solution.py:482
  19.1 0.0 copy-start.5
  19.1 0.0 copy-start.2
  19.1 0.0 copy-start.3
  19.1 4.2 %attend.1 = bf16[16,2,512]{2,1,0:T(2,128)(2,1)S(1)} custom-call(s32[2]{0:T(128)} %lengths_hbm.3, bf16[16,2,544]{2,1,0:T(2,128)(2,1)S(1)} %all_to_all.35.query_ref, f32[4,32]{1,0:T(4,128)S(1)} %get-tuple-element.19.trig_ref, bf16[2,4096,512]{2,1,0:T(8,128)(2,1)} %latent_hbm.1, bf16[2,32,4096]{2,1,0:T(8,128)(2,1)} %rotary_hbm.1), custom_call_target="tpu_custom_call" | custom-call | flops 268435456 | tf_op jit(solution)/shard_map/attend/pallas_call | solution.py:23
  23.3 0.0 copy-start.1
  23.3 11.3 %all_to_all.36 = bf16[16,2,512]{2,1,0:T(2,128)(2,1)S(1)} all-to-all(bf16[16,2,512]{2,1,0:T(2,128)(2,1)S(1)} %attend.1), channel_id=1, replica_groups=mesh['ep'=16,'tp'=16] {'tp'}, dimensions={0} | all-to-all | bytes 65536 | tf_op jit(solution)/shard_map/all_to_all | solution.py:482
  34.6 0.0 copy-done
  34.6 0.0 copy-done.5
  34.7 0.3 convolution_convert_fusion
  35.0 0.1 reshape.31
  35.1 12.0 %all_to_all.37 = bf16[16,2,2048]{2,1,0:T(2,128)(2,1)S(1)} all-to-all(bf16[16,2,2048]{2,1,0:T(2,128)(2,1)S(1)} %reshape.31), channel_id=1, replica_groups=mesh['ep'=16,'tp'=16] {'tp'}, dimensions={0} | all-to-all | bytes 262144 | tf_op jit(solution)/shard_map/all_to_all | solution.py:482
  47.1 0.1 reshape.32.terms_ref
  47.1 0.0 copy-done.2
  47.1 0.0 copy-done.3
  47.1 0.4 mix.1
  47.5 10.2 %all_to_all.38 = bf16[16,2,1024]{2,1,0:T(2,128)(2,1)S(1)} all-to-all(bf16[16,2,1024]{2,1,0:T(2,128)(2,1)S(1)} %get-tuple-element.21), channel_id=1, replica_groups=mesh['ep'=16,'tp'=16] {'tp'}, dimensions={0} | all-to-all | bytes 131072 | tf_op jit(solution)/shard_map/all_to_all | solution.py:482
  57.7 0.2 dispatch.1
  57.9 14.6 %all_to_all.39 = bf16[16,8,1024]{2,1,0:T(8,128)(2,1)S(1)} all-to-all(bf16[16,8,1024]{2,1,0:T(8,128)(2,1)S(1)} %bitcast.29), channel_id=1, replica_groups=mesh['ep'=16,'tp'=16] {'ep'}, dimensions={0} | all-to-all | bytes 524288 | tf_op jit(solution)/shard_map/all_to_all | solution.py:482
  72.5 1.3 %collective-permute-start = (bf16[128,1024]{1,0:T(8,128)(2,1)S(1)}, bf16[128,1024]{1,0:T(8,128)(2,1)S(1)}, u32[]{:S(2)}, u32[]{:S(2)}) collective-permute-start(bf16[128,1024]{1,0:T(8,128)(2,1)S(1)} %bitcast.31), channel_id=1, source_target_pairs={{0,1},{1,0},{2,3},{3,2},{4,5},{5,4},{6,7},{7,6},{8,9},{9,8},{10,11... | collective-permute-start | bytes 786440 | tf_op jit(solution)/shard_map/ppermute | solution.py:449
  73.8 0.0 copy-done.1
  73.8 1.7 %enter.1 = (f32[128,448]{1,0:T(8,128)S(1)}, f32[128,448]{1,0:T(8,128)S(1)}) custom-call(bf16[128,1024]{1,0:T(8,128)(2,1)S(1)} %bitcast.32, bf16[448,2048]{1,0:T(8,128)(2,1)S(1)} %bitcast.27, bf16[448,2048]{1,0:T(8,128)(2,1)} %bitcast.36), custom_call_target="tpu_custom_call" | custom-call | flops 234881024 | tf_op jit(solution)/shard_map/enter/pallas_call | solution.py:23
  75.5 0.0 collective-permute-done.rows_ref
  75.5 2.2 %leave.1 = (bf16[128,448]{1,0:T(8,128)(2,1)S(1)}, bf16[128,1024]{1,0:T(8,128)(2,1)S(1)}) custom-call(bf16[128,1024]{1,0:T(8,128)(2,1)S(1)} %collective-permute-done.rows_ref, bf16[448,2048]{1,0:T(8,128)(2,1)S(1)} %bitcast.28, bf16[448,2048]{1,0:T(8,128)(2,1)} %bitcast.37, bf16[448,2048]{1,0:T(8,128)(2,1)} %bitcast.38, ...), custom_call_target="tpu_custom_call" | custom-call | flops 352321536 | tf_op jit(solution)/shard_map/leave/pallas_call | solution.py:23
  77.7 0.1 collective-permute-start.1
  77.8 0.0 copy-start.4
  77.8 1.5 %close.1 = f32[128,1024]{1,0:T(8,128)S(1)} custom-call(bf16[128,448]{1,0:T(8,128)(2,1)S(1)} %get-tuple-element.24.act_ref, bf16[448,2048]{1,0:T(8,128)(2,1)} %bitcast.39), custom_call_target="tpu_custom_call" | custom-call | flops 117440512 | tf_op jit(solution)/shard_map/close/pallas_call | solution.py:23
  79.3 0.0 collective-permute-done.1
  79.3 0.1 fusion
  79.4 10.7 %all_to_all.40 = bf16[16,8,1024]{2,1,0:T(8,128)(2,1)S(1)} all-to-all(bf16[16,8,1024]{2,1,0:T(8,128)(2,1)S(1)} %fusion), channel_id=1, replica_groups=mesh['ep'=16,'tp'=16] {'ep'}, dimensions={0} | all-to-all | bytes 524288 | tf_op jit(solution)/shard_map/all_to_all | solution.py:482
  90.1 0.3 combine.1
  90.4 11.8 %all_to_all.41 = bf16[16,2,1024]{2,1,0:T(2,128)(2,1)S(1)} all-to-all(bf16[16,2,1024]{2,1,0:T(2,128)(2,1)S(1)} %reshape.38), channel_id=1, replica_groups=mesh['ep'=16,'tp'=16] {'tp'}, dimensions={0} | all-to-all | bytes 131072 | tf_op jit(solution)/shard_map/all_to_all | solution.py:482
  102.3 0.0 copy-done.4
  102.3 0.9 finish.1
  (4 shorter events, 0.1 us)
Async XLA Ops:
  0.0 34.6 %copy-start = (bf16[64,2048]{1,0:T(8,128)(2,1)S(1)}, bf16[64,2048]{1,0:T(8,128)(2,1)}, u32[]{:S(2)}) copy-start(bf16[64,2048]{1,0:T(8,128)(2,1)} %param.27) | copy-start | bytes 786436
  19.1 15.6 %copy-start.5 = (bf16[1,512,64]{1,2,0:T(8,128)(2,1)S(1)}, bf16[1,512,64]{1,2,0:T(8,128)(2,1)}, u32[]{:S(2)}) copy-start(bf16[1,512,64]{1,2,0:T(8,128)(2,1)} %param.26) | copy-start | bytes 196612
  19.1 28.0 %copy-start.2 = (f32[2048]{0:T(1024)S(1)}, f32[2048]{0:T(1024)}, u32[]{:S(2)}) copy-start(f32[2048]{0:T(1024)} %param.28) | copy-start | bytes 24580
  19.1 28.0 %copy-start.3 = (f32[2048]{0:T(1024)S(1)}, f32[2048]{0:T(1024)}, u32[]{:S(2)}) copy-start(f32[2048]{0:T(1024)} %param.29) | copy-start | bytes 24580
  23.3 50.5 %copy-start.1 = (bf16[1,2048,448]{1,2,0:T(8,128)(2,1)S(1)}, bf16[1,2048,448]{1,2,0:T(8,128)(2,1)}, u32[]{:S(2)}) copy-start(bf16[1,2048,448]{1,2,0:T(8,128)(2,1)} %param.32) | copy-start | bytes 5505028
  72.5 2.9 %collective-permute-start = (bf16[128,1024]{1,0:T(8,128)(2,1)S(1)}, bf16[128,1024]{1,0:T(8,128)(2,1)S(1)}, u32[]{:S(2)}, u32[]{:S(2)}) collective-permute-start(bf16[128,1024]{1,0:T(8,128)(2,1)S(1)} %bitcast.31), channel_id=1, source_target_pairs={{0,1},{1,0},{2,3},{3,2},{4,5},{5,4},{6,7},{7,6},{8,9},{9,8},{10,11... | collective-permute-start | bytes 786440 | tf_op jit(solution)/shard_map/ppermute | solution.py:449
  77.7 1.6 %collective-permute-start.1 = (bf16[128,1024]{1,0:T(8,128)(2,1)S(1)}, bf16[128,1024]{1,0:T(8,128)(2,1)S(1)}, u32[]{:S(2)}, u32[]{:S(2)}) collective-permute-start(bf16[128,1024]{1,0:T(8,128)(2,1)S(1)} %get-tuple-element.25), channel_id=1, source_target_pairs={{0,1},{1,0},{2,3},{3,2},{4,5},{5,4},{6,7},{7,6},{8,9},{9,8},{10,11... | collective-permute-start | bytes 786440 | tf_op jit(solution)/shard_map/ppermute | solution.py:468
  77.8 24.5 %copy-start.4 = (f32[2048]{0:T(1024)S(1)}, f32[2048]{0:T(1024)}, u32[]{:S(2)}) copy-start(f32[2048]{0:T(1024)} %param.35) | copy-start | bytes 24580

commit v3 on v2

--- a/solution.py
+++ b/solution.py
@@ -14,8 +14,9 @@
 VMEM = pl.BlockSpec(memory_space=pltpu.VMEM)
 SMEM = pl.BlockSpec(memory_space=pltpu.SMEM)
 HBM = pl.BlockSpec(memory_space=pltpu.HBM)
-ATTEND_LIMIT = 14 * 1024 * 1024
-SMALL_LIMIT = 8 * 1024 * 1024
+AHEAD = 10**10
+ATTEND_LIMIT = 2 * 1024 * 1024
+SMALL_LIMIT = 4 * 1024 * 1024
 NT = (((1,), (1,)), ((), ()))
 
 
@@ -110,6 +111,8 @@
         turned = jnp.sin(angles)
         trig_ref[2 * s : 2 * s + 1, :] = jnp.cos(angles)
         trig_ref[2 * s + 1 : 2 * s + 2, :] = jnp.where(lane < half, -turned, turned)
+        at = 2 * own_rows + s
+        trig_ref[at : at + 1, :] = jnp.zeros_like(angles) + lengths_ref[s].astype(jnp.float32)
 
     copies[3].wait()
     copies[4].wait()
@@ -137,7 +140,9 @@
     return tuple(pltpu.with_memory_space_constraint(a, pltpu.HBM) for a in arrays)
 
 
-def front(hidden, gain, query_weight, rotary_weight, key_up, ids, logits, lengths, peers, capacity):
+def front(
+    hidden, gain, query_weight, rotary_weight, key_up, ids, logits, lengths, peers, capacity,
+):
     rows, features = hidden.shape
     own_rows = rows // peers
     rope, latent = rotary_weight.shape[1], key_up.shape[1]
@@ -153,65 +158,53 @@
             shape((own_rows, features), jnp.bfloat16),
             shape((2, rows), jnp.float32),
             shape((rows, 4), jnp.float32),
-            shape((2 * own_rows, rope), jnp.float32),
+            shape((3 * own_rows, rope), jnp.float32),
         ),
         [HBM] * 8,
         arrays,
         scratch=held + [pltpu.SMEM(lengths.shape, lengths.dtype), pltpu.SemaphoreType.DMA((8,))],
+        flops=AHEAD,
     )
 
 
 def attend_kernel(
-    scale, lengths_hbm, query_ref, trig_ref, latent_hbm, rotary_hbm, out_ref,
-    lengths_ref, latent_ref, rotary_ref, latent_query, rotary_query, summed_ref,
-    lengths_sem, latent_sems, rotary_sems,
+    scale, query_ref, trig_ref, latent_ref, rope_ref, out_ref, latent_query, rotary_query, summed_ref
 ):
-    heads, rows, _ = query_ref.shape
-    width, rope = latent_query.shape[2], rotary_query.shape[2]
-    most = latent_hbm.shape[1] // BLOCK
-
-    def copies(s, b):
-        at = pl.ds(b * BLOCK, BLOCK)
-        return (
-            pltpu.make_async_copy(
-                latent_hbm.at[s, at, :], latent_ref.at[s, at, :], latent_sems.at[s, b]
-            ),
-            pltpu.make_async_copy(
-                rotary_hbm.at[s, :, at], rotary_ref.at[s, :, at], rotary_sems.at[s, b]
-            ),
-        )
-
-    fetch = pltpu.make_async_copy(lengths_hbm, lengths_ref, lengths_sem)
-    fetch.start()
-    for s in range(rows):
-        for copy in copies(s, 0):
-            copy.start()
+    rows, heads, width = latent_query.shape
+    rope = rotary_query.shape[2]
+    most = latent_ref.shape[1] // BLOCK
+    lengths = [
+        jnp.max(trig_ref[2 * rows + s : 2 * rows + s + 1, :]).astype(jnp.int32) for s in range(rows)
+    ]
+    counts = [lax.div(length + (BLOCK - 1), BLOCK) for length in lengths]
+
+    place = lax.broadcasted_iota(jnp.int32, (rows * heads, rows * heads), 0)
+    other = lax.broadcasted_iota(jnp.int32, (rows * heads, rows * heads), 1)
+    by_head = jnp.where(lax.rem(place, rows) * heads + lax.div(place, rows) == other, 1.0, 0.0)
     swap = lax.broadcasted_iota(jnp.int32, (rope, rope), 0) == lax.rem(
         lax.broadcasted_iota(jnp.int32, (rope, rope), 1) + rope // 2, rope
     )
     swap = jnp.where(swap, 1.0, 0.0).astype(jnp.bfloat16)
-    query = query_ref[...].astype(jnp.float32)
+    received = query_ref[...].astype(jnp.float32)
+    query = jnp.concatenate(
+        [received[h, s : s + 1, :] for s in range(rows) for h in range(heads)], axis=0
+    )
+    plain = query[:, width:]
+    turned = jnp.dot(plain.astype(jnp.bfloat16), swap, preferred_element_type=jnp.float32)
     for s in range(rows):
-        own = jnp.concatenate([query[h, s : s + 1, :] for h in range(heads)], axis=0)
-        latent_query[s] = own[:, :width].astype(jnp.bfloat16)
-        plain = own[:, width:]
-        turned = jnp.dot(plain.astype(jnp.bfloat16), swap, preferred_element_type=jnp.float32)
+        at = slice(s * heads, (s + 1) * heads)
+        latent_query[s] = query[at, :width].astype(jnp.bfloat16)
         rotary_query[s] = (
-            plain * trig_ref[2 * s : 2 * s + 1, :] + turned * trig_ref[2 * s + 1 : 2 * s + 2, :]
+            plain[at] * trig_ref[2 * s : 2 * s + 1, :]
+            + turned[at] * trig_ref[2 * s + 1 : 2 * s + 2, :]
         ).astype(jnp.bfloat16)
-    fetch.wait()
-    for s in range(rows):
-        blocks = lax.div(lengths_ref[s] + (BLOCK - 1), BLOCK)
-        for b in range(1, most):
-
-            @pl.when(b < blocks)
-            def _start(s=s, b=b):
-                for copy in copies(s, b):
-                    copy.start()
+
+    first = jnp.where(counts[0] <= counts[1], 0, 1)
 
     @pl.loop(0, rows)
-    def _sequence(s):
-        length = lengths_ref[s]
+    def _sequence(i):
+        s = jnp.where(i == 0, first, 1 - first)
+        length = jnp.where(s == 0, lengths[0], lengths[1])
         blocks = lax.div(length + (BLOCK - 1), BLOCK)
         for count in range(1, most + 1):
 
@@ -220,14 +213,13 @@
                 scores = []
                 for b in range(count):
                     at = slice(b * BLOCK, (b + 1) * BLOCK)
-                    for copy in copies(s, b):
-                        copy.wait()
                     part = lax.dot_general(
                         latent_query[s], latent_ref[s, at, :], NT,
                         preferred_element_type=jnp.float32,
                     )
                     part = part + jnp.dot(
-                        rotary_query[s], rotary_ref[s, :, at], preferred_element_type=jnp.float32
+                        rotary_query[s], rope_ref[s, :, at],
+                        preferred_element_type=jnp.float32,
                     )
                     part = part * scale
                     if b == count - 1:
@@ -246,41 +238,33 @@
                 summed = None
                 for b in range(count):
                     probs = (weights[b] * factor).astype(jnp.bfloat16)
+                    at = slice(b * BLOCK, (b + 1) * BLOCK)
                     term = jnp.dot(
-                        probs, latent_ref[s, b * BLOCK : (b + 1) * BLOCK, :],
+                        probs, latent_ref[s, at, :],
                         preferred_element_type=jnp.float32,
                     )
                     summed = term if summed is None else summed + term
-                summed_ref[s] = summed
-
-    sums = [summed_ref[s] for s in range(rows)]
-    for h in range(heads):
-        out_ref[h] = jnp.concatenate([part[h : h + 1, :] for part in sums], axis=0).astype(
-            jnp.bfloat16
-        )
-
-
-def attend(query, trig, latent, rotary, lengths, scale):
-    heads, rows, _ = query.shape
-    width, rope = latent.shape[2], rotary.shape[1]
-    blocks = latent.shape[1] // BLOCK
-    lengths, latent, rotary = in_hbm(lengths, latent, rotary)
+                summed_ref[s] = summed.astype(jnp.bfloat16)
+
+    sums = jnp.concatenate([summed_ref[s] for s in range(rows)], axis=0)
+    out_ref[...] = jnp.dot(
+        by_head.astype(jnp.bfloat16), sums, preferred_element_type=jnp.float32
+    ).astype(jnp.bfloat16)
+
+
+def attend(query, trig, latent, rotary, scale):
+    rows, most, width = latent.shape
+    heads, rope = query.shape[0], rotary.shape[1]
     return call(
         functools.partial(attend_kernel, scale),
         "attend",
-        shape((heads, rows, width), jnp.bfloat16),
-        [HBM, VMEM, VMEM, HBM, HBM],
-        (lengths, query, trig, latent, rotary),
+        shape((heads * rows, width), jnp.bfloat16),
+        [VMEM] * 4,
+        (query, trig, latent, rotary),
         scratch=(
-            pltpu.SMEM(lengths.shape, lengths.dtype),
-            pltpu.VMEM(latent.shape, latent.dtype),
-            pltpu.VMEM(rotary.shape, rotary.dtype),
             pltpu.VMEM((rows, heads, width), jnp.bfloat16),
             pltpu.VMEM((rows, heads, rope), jnp.bfloat16),
-            pltpu.VMEM((rows, heads, width), jnp.float32),
-            pltpu.SemaphoreType.DMA,
-            pltpu.SemaphoreType.DMA((rows, blocks)),
-            pltpu.SemaphoreType.DMA((rows, blocks)),
+            pltpu.VMEM((rows, heads, width), jnp.bfloat16),
         ),
         limit=ATTEND_LIMIT,
         flops=4 * latent.size * heads,
@@ -337,6 +321,7 @@
         shape((slots, rows.shape[1]), jnp.bfloat16),
         [VMEM] * 2,
         (own_slots, rows),
+        flops=AHEAD,
     )
 
 
@@ -399,70 +384,49 @@
     return lax.dot_general(rows, weight, NT, preferred_element_type=jnp.float32)
 
 
-def enter_kernel(rows_ref, gate_ref, up_hbm, gate_out, up_out, up_ref, sem):
-    half = rows_ref.shape[1]
-    at = half_at(True, half)
-    copy = pltpu.make_async_copy(up_hbm.at[:, at], up_ref, sem)
-    copy.start()
+def enter_kernel(rows_ref, gate_ref, up_ref, gate_out, up_out):
     rows = rows_ref[...]
+    at = half_at(True, rows.shape[1])
     gate_out[...] = product(rows, gate_ref[:, at])
-    copy.wait()
-    up_out[...] = product(rows, up_ref[...])
-
-
-def leave_kernel(
-    rows_ref, gate_ref, up_hbm, down_hbm, gate_part, up_part, act_ref, out_ref, up_ref, down_ref, sems
-):
-    half = rows_ref.shape[1]
-    at = half_at(False, half)
-    copies = [
-        pltpu.make_async_copy(up_hbm.at[:, at], up_ref, sems.at[0]),
-        pltpu.make_async_copy(down_hbm.at[:, at], down_ref, sems.at[1]),
-    ]
-    for copy in copies:
-        copy.start()
+    up_out[...] = product(rows, up_ref[:, at])
+
+
+def leave_kernel(rows_ref, gate_ref, up_ref, down_ref, gate_part, up_part, act_ref, out_ref):
     rows = rows_ref[...]
+    at = half_at(False, rows.shape[1])
     gate = gate_part[...] + product(rows, gate_ref[:, at])
-    copies[0].wait()
-    up = up_part[...] + product(rows, up_ref[...])
+    up = up_part[...] + product(rows, up_ref[:, at])
     act = (gate / (1.0 + jnp.exp(-gate)) * up).astype(jnp.bfloat16)
     act_ref[...] = act
-    copies[1].wait()
-    out_ref[...] = jnp.dot(act, down_ref[...], preferred_element_type=jnp.float32).astype(
+    out_ref[...] = jnp.dot(act, down_ref[:, at], preferred_element_type=jnp.float32).astype(
         jnp.bfloat16
     )
 
 
-def close_kernel(act_ref, down_hbm, out_ref, down_ref, sem):
-    copy = pltpu.make_async_copy(down_hbm.at[:, half_at(True, out_ref.shape[1])], down_ref, sem)
-    copy.start()
-    copy.wait()
-    out_ref[...] = jnp.dot(act_ref[...], down_ref[...], preferred_element_type=jnp.float32)
+def close_kernel(act_ref, down_ref, out_ref):
+    at = half_at(True, out_ref.shape[1])
+    out_ref[...] = jnp.dot(act_ref[...], down_ref[:, at], preferred_element_type=jnp.float32)
 
 
 def expert_rows(rows, gate_weight, up_weight, down_weight, pairs):
     slots, half = rows.shape
     width = gate_weight.shape[0]
-    up_weight, down_weight = in_hbm(up_weight, down_weight)
     part = shape((slots, width), jnp.float32)
-    side = pltpu.VMEM((width, half), jnp.bfloat16)
     other = lax.ppermute(rows, "tp", pairs)
     gate_part, up_part = call(
         enter_kernel,
         "enter",
         (part, part),
-        [VMEM, VMEM, HBM],
+        [VMEM] * 3,
         (rows, gate_weight, up_weight),
-        scratch=(side, pltpu.SemaphoreType.DMA),
         flops=4 * slots * half * width,
     )
     act, sent = call(
         leave_kernel,
         "leave",
         (shape((slots, width), jnp.bfloat16), shape((slots, half), jnp.bfloat16)),
-        [VMEM, VMEM, HBM, HBM, VMEM, VMEM],
+        [VMEM] * 6,
         (other, gate_weight, up_weight, down_weight, gate_part, up_part),
-        scratch=(side, side, pltpu.SemaphoreType.DMA((2,))),
         flops=6 * slots * half * width,
     )
     arrived = lax.ppermute(sent, "tp", pairs)
@@ -470,9 +434,8 @@
         close_kernel,
         "close",
         shape((slots, half), jnp.float32),
-        [VMEM, HBM],
+        [VMEM] * 2,
         (act, down_weight),
-        scratch=(side, pltpu.SemaphoreType.DMA),
         flops=2 * slots * half * width,
     )
     return (kept + arrived.astype(jnp.float32)).astype(jnp.bfloat16)
@@ -527,8 +490,11 @@
     )
     query = exchanged(query, "tp")
     score_scale = (nope_width + rotary_width) ** (-0.5)
-    out_latent = attend(query, trig, cache_latent, cache_rotary, lengths, score_scale)
-    out_latent = exchanged(out_latent, "tp").reshape(group_rows, latent_width)
+    out_latent = attend(
+        query, trig, cache_latent, cache_rotary, score_scale
+    )
+    out_latent = exchanged(out_latent.reshape(peers, own_rows, latent_width), "tp")
+    out_latent = out_latent.reshape(group_rows, latent_width)
     head_out = jnp.dot(out_latent, value_up[0], preferred_element_type=jnp.float32)
     head_terms = jnp.dot(
         head_out.astype(jnp.bfloat16), out_weight, preferred_element_type=jnp.float32

time: 104 us -> 101 us (0.971)
  Pallas kernels: 13.1 us -> 7.53 us
  waiting for transfers between devices: 0.01 us -> 1.66 us
    pallas_call x9, Pallas kernels: 13.1 us -> 7.53 us  [call(): pl.pallas_call(kernel, out_shape=outs, in_specs=ins, out_specs=jax.tree.m...]
    ppermute x1, waiting for transfers between devices: 0.01 us -> 1.19 us  [expert_rows(): arrived = lax.ppermute(sent, 'tp', pairs)]
  transfers between devices with their start and end apart: 2 -> 2, of which waited for: 0 -> 2; matrix products, arithmetic and copies ran while one was open for 0% -> 0% of each run, Pallas kernels for 3% -> 1%
where the time goes in v3:
time: 101 us; the launch traced here: 100 us
  blocking collectives  88.4 us (88%)
  Pallas kernels  7.53 us (7%)
  waiting for transfers between devices  1.66 us (2%)
  starting transfers between devices  1.38 us (1%)
    all_to_all x7, blocking collectives, exchanged(): return lax.all_to_all(array, axis, split_axis=0, concat_axis=0, tiled=True)  88.4 us
    pallas_call x9, Pallas kernels, call(): pl.pallas_call(kernel, out_shape=outs, in_specs=ins, out_specs=jax.tree.m...  7.53 us
  transfers between devices with their start and end apart: 2, of which 2 were waited for; matrix products, arithmetic and copies ran while one was open for 0% of the time, Pallas kernels for 1%

profile of v3, /device:TPU:1, one launch (start us, length us, event | category | flops | bytes accessed | tf_op | source)
XLA Modules:
  0.0 100.3 jit_solution(4003284997349321356)
XLA Ops:
  0.0 0.0 copy-start
  0.0 0.0 slice-start
  0.0 0.0 slice-start.1
  0.0 0.0 copy-start.4
  0.0 2.0 %front.1 = (bf16[16,2,544]{2,1,0:T(2,128)(2,1)S(1)}, bf16[2,2048]{1,0:T(2,128)(2,1)S(1)}, f32[2,32]{1,0:T(2,128)S(1)}, f32[32,4]{1,0:T(8,128)S(1)}, f32[6,32]{1,0:T(8,128)S(1)}) custom-call(bf16[32,2048]{1,0:T(8,128)(2,1)} %hidden_hbm.1, f32[1,2048]{1,0:T(1,128)} %bitcast.45, bf16[64,2048]{1,0:T(8,128)(2,1)} %bitcast.42, bf16[32,2048]{1,0:T(8,128)(2,1)} %bitcast.43, ...), custom_call_target="tpu_custom_call" | custom-call | flops 10000000000 | tf_op jit(solution)/shard_map/front/pallas_call | solution.py:24
  2.0 17.4 %all_to_all.35.query_ref = bf16[16,2,544]{2,1,0:T(2,128)(2,1)S(1)} all-to-all(bf16[16,2,544]{2,1,0:T(2,128)(2,1)S(1)} %get-tuple-element.18), channel_id=1, replica_groups=mesh['ep'=16,'tp'=16] {'tp'}, dimensions={0} | all-to-all | bytes 69632 | tf_op jit(solution)/shard_map/all_to_all | solution.py:445
  19.5 0.0 slice-done
  19.5 0.0 slice-done.1
  19.5 0.0 copy-done.4
  19.5 0.0 copy-start.8
  19.5 0.0 copy-start.5
  19.5 0.0 copy-start.6
  19.5 1.9 %attend.1 = bf16[32,512]{1,0:T(8,128)(2,1)S(1)} custom-call(bf16[16,2,544]{2,1,0:T(2,128)(2,1)S(1)} %all_to_all.35.query_ref, f32[6,32]{1,0:T(8,128)S(1)} %get-tuple-element.19.trig_ref, bf16[2,4096,512]{2,1,0:T(8,128)(2,1)S(1)} %bitcast.28, bf16[2,32,4096]{2,1,0:T(8,128)(2,1)S(1)} %copy-done.4), custom_call_target="tpu_custom_call" | custom-call | flops 268435456 | tf_op jit(solution)/shard_map/attend/pallas_call | solution.py:24
  21.5 10.8 %all_to_all.36 = bf16[16,2,512]{2,1,0:T(2,128)(2,1)S(1)} all-to-all(bf16[16,2,512]{2,1,0:T(2,128)(2,1)S(1)} %reshape.33), channel_id=1, replica_groups=mesh['ep'=16,'tp'=16] {'tp'}, dimensions={0} | all-to-all | bytes 65536 | tf_op jit(solution)/shard_map/all_to_all | solution.py:445
  32.3 0.0 copy-done
  32.3 0.0 copy-done.8
  32.3 0.3 convolution_convert_fusion
  32.6 0.1 reshape.35
  32.8 12.0 %all_to_all.37 = bf16[16,2,2048]{2,1,0:T(2,128)(2,1)S(1)} all-to-all(bf16[16,2,2048]{2,1,0:T(2,128)(2,1)S(1)} %reshape.35), channel_id=1, replica_groups=mesh['ep'=16,'tp'=16] {'tp'}, dimensions={0} | all-to-all | bytes 262144 | tf_op jit(solution)/shard_map/all_to_all | solution.py:445
  44.7 0.1 reshape.36.terms_ref
  44.8 0.0 copy-done.5
  44.8 0.0 copy-done.6
  44.8 0.4 mix.1
  45.2 10.2 %all_to_all.38 = bf16[16,2,1024]{2,1,0:T(2,128)(2,1)S(1)} all-to-all(bf16[16,2,1024]{2,1,0:T(2,128)(2,1)S(1)} %get-tuple-element.21), channel_id=1, replica_groups=mesh['ep'=16,'tp'=16] {'tp'}, dimensions={0} | all-to-all | bytes 131072 | tf_op jit(solution)/shard_map/all_to_all | solution.py:445
  55.4 0.0 copy-start.1
  55.4 0.0 copy-start.2
  55.4 0.2 dispatch.1
  55.6 15.5 %all_to_all.39 = bf16[16,8,1024]{2,1,0:T(8,128)(2,1)S(1)} all-to-all(bf16[16,8,1024]{2,1,0:T(8,128)(2,1)S(1)} %bitcast.38), channel_id=1, replica_groups=mesh['ep'=16,'tp'=16] {'ep'}, dimensions={0} | all-to-all | bytes 524288 | tf_op jit(solution)/shard_map/all_to_all | solution.py:445
  71.2 1.3 %collective-permute-start = (bf16[128,1024]{1,0:T(8,128)(2,1)S(1)}, bf16[128,1024]{1,0:T(8,128)(2,1)S(1)}, u32[]{:S(2)}, u32[]{:S(2)}) collective-permute-start(bf16[128,1024]{1,0:T(8,128)(2,1)S(1)} %bitcast.36), channel_id=1, source_target_pairs={{0,1},{1,0},{2,3},{3,2},{4,5},{5,4},{6,7},{7,6},{8,9},{9,8},{10,11... | collective-permute-start | bytes 786440 | tf_op jit(solution)/shard_map/ppermute | solution.py:415
  72.4 0.0 copy-done.1
  72.4 0.0 copy-done.2
  72.4 0.0 copy-start.3
  72.4 0.7 enter.1
  73.1 0.5 collective-permute-done.rows_ref
  73.6 0.3 copy-done.3
  73.9 0.9 leave.1
  74.9 0.1 collective-permute-start.1
  75.0 0.0 copy-start.7
  75.0 0.3 close.1
  75.3 1.2 %collective-permute-done.1 = bf16[128,1024]{1,0:T(8,128)(2,1)S(1)} collective-permute-done((bf16[128,1024]{1,0:T(8,128)(2,1)S(1)}, bf16[128,1024]{1,0:T(8,128)(2,1)S(1)}, u32[]{:S(2)}, u32[]{:S(2)}) %collective-permute-start.1) | collective-permute-done | bytes 262176 | tf_op jit(solution)/shard_map/ppermute | solution.py:432
  76.5 0.1 fusion
  76.6 11.0 %all_to_all.40 = bf16[16,8,1024]{2,1,0:T(8,128)(2,1)S(1)} all-to-all(bf16[16,8,1024]{2,1,0:T(8,128)(2,1)S(1)} %fusion), channel_id=1, replica_groups=mesh['ep'=16,'tp'=16] {'ep'}, dimensions={0} | all-to-all | bytes 524288 | tf_op jit(solution)/shard_map/all_to_all | solution.py:445
  87.5 0.3 combine.1
  87.9 11.5 %all_to_all.41 = bf16[16,2,1024]{2,1,0:T(2,128)(2,1)S(1)} all-to-all(bf16[16,2,1024]{2,1,0:T(2,128)(2,1)S(1)} %reshape.42), channel_id=1, replica_groups=mesh['ep'=16,'tp'=16] {'tp'}, dimensions={0} | all-to-all | bytes 131072 | tf_op jit(solution)/shard_map/all_to_all | solution.py:445
  99.4 0.0 copy-done.7
  99.4 0.8 finish.1
  (6 shorter events, 0.1 us)
Async XLA Ops:
  0.0 32.3 %copy-start = (bf16[64,2048]{1,0:T(8,128)(2,1)S(1)}, bf16[64,2048]{1,0:T(8,128)(2,1)}, u32[]{:S(2)}) copy-start(bf16[64,2048]{1,0:T(8,128)(2,1)} %param.27) | copy-start | bytes 786436
  0.0 19.5 %slice-start = ((s8[8388608]{0:T(1024)(128)(4,1)}), s8[4194304]{0:T(1024)(128)(4,1)S(1)}, s32[]{:S(2)}) async-start(s8[8388608]{0:T(1024)(128)(4,1)} %bitcast.27), calls=%async_computation.7 | async-start | bytes 8388608
  0.0 19.5 %slice-start.1 = ((s8[8388608]{0:T(1024)(128)(4,1)}), s8[4194304]{0:T(1024)(128)(4,1)S(1)}, s32[]{:S(2)}) async-start(s8[8388608]{0:T(1024)(128)(4,1)} %bitcast.27), calls=%async_computation.8 | async-start | bytes 8388608
  0.0 19.5 %copy-start.4 = (bf16[2,32,4096]{2,1,0:T(8,128)(2,1)S(1)}, bf16[2,32,4096]{2,1,0:T(8,128)(2,1)}, u32[]{:S(2)}) copy-start(bf16[2,32,4096]{2,1,0:T(8,128)(2,1)} %rope_ref.1) | copy-start | bytes 1572868
  19.5 12.8 %copy-start.8 = (bf16[1,512,64]{1,2,0:T(8,128)(2,1)S(1)}, bf16[1,512,64]{1,2,0:T(8,128)(2,1)}, u32[]{:S(2)}) copy-start(bf16[1,512,64]{1,2,0:T(8,128)(2,1)} %param.26) | copy-start | bytes 196612
  19.5 25.3 %copy-start.5 = (f32[2048]{0:T(1024)S(1)}, f32[2048]{0:T(1024)}, u32[]{:S(2)}) copy-start(f32[2048]{0:T(1024)} %param.28) | copy-start | bytes 24580
  19.5 25.3 %copy-start.6 = (f32[2048]{0:T(1024)S(1)}, f32[2048]{0:T(1024)}, u32[]{:S(2)}) copy-start(f32[2048]{0:T(1024)} %param.29) | copy-start | bytes 24580
  55.4 17.0 %copy-start.1 = (bf16[1,2048,448]{1,2,0:T(8,128)(2,1)S(1)}, bf16[1,2048,448]{1,2,0:T(8,128)(2,1)}, u32[]{:S(2)}) copy-start(bf16[1,2048,448]{1,2,0:T(8,128)(2,1)} %param.32) | copy-start | bytes 5505028
  55.4 17.0 %copy-start.2 = (bf16[1,2048,448]{1,2,0:T(8,128)(2,1)S(1)}, bf16[1,2048,448]{1,2,0:T(8,128)(2,1)}, u32[]{:S(2)}) copy-start(bf16[1,2048,448]{1,2,0:T(8,128)(2,1)} %param.33) | copy-start | bytes 5505028
  71.2 2.4 %collective-permute-start = (bf16[128,1024]{1,0:T(8,128)(2,1)S(1)}, bf16[128,1024]{1,0:T(8,128)(2,1)S(1)}, u32[]{:S(2)}, u32[]{:S(2)}) collective-permute-start(bf16[128,1024]{1,0:T(8,128)(2,1)S(1)} %bitcast.36), channel_id=1, source_target_pairs={{0,1},{1,0},{2,3},{3,2},{4,5},{5,4},{6,7},{7,6},{8,9},{9,8},{10,11... | collective-permute-start | bytes 786440 | tf_op jit(solution)/shard_map/ppermute | solution.py:415
  72.4 1.5 %copy-start.3 = (bf16[1,448,2048]{2,1,0:T(8,128)(2,1)S(1)}, bf16[1,448,2048]{2,1,0:T(8,128)(2,1)}, u32[]{:S(2)}) copy-start(bf16[1,448,2048]{2,1,0:T(8,128)(2,1)} %param.34) | copy-start | bytes 5505028
  74.9 1.6 %collective-permute-start.1 = (bf16[128,1024]{1,0:T(8,128)(2,1)S(1)}, bf16[128,1024]{1,0:T(8,128)(2,1)S(1)}, u32[]{:S(2)}, u32[]{:S(2)}) collective-permute-start(bf16[128,1024]{1,0:T(8,128)(2,1)S(1)} %get-tuple-element.25), channel_id=1, source_target_pairs={{0,1},{1,0},{2,3},{3,2},{4,5},{5,4},{6,7},{7,6},{8,9},{9,8},{10,11... | collective-permute-start | bytes 786440 | tf_op jit(solution)/shard_map/ppermute | solution.py:432
  75.0 24.4 %copy-start.7 = (f32[2048]{0:T(1024)S(1)}, f32[2048]{0:T(1024)}, u32[]{:S(2)}) copy-start(f32[2048]{0:T(1024)} %param.35) | copy-start | bytes 24580

commit v4 on v3

--- a/solution.py
+++ b/solution.py
@@ -73,9 +73,8 @@
     for copy in copies:
         copy.start()
     group, place = lax.axis_index("ep"), lax.axis_index("tp")
-
-    copies[1].wait()
-    copies[2].wait()
+    for copy in copies:
+        copy.wait()
     ids_all = ids_ref[...].astype(jnp.float32)
     logits_all = logits_ref[...]
     ids = jnp.zeros((2, group_rows), jnp.float32)
@@ -99,7 +98,6 @@
         columns_ref[:, k : k + 1] = column(slot)
         columns_ref[:, 2 + k : 3 + k] = column(weights[k] / (weights[0] + weights[1]))
 
-    copies[0].wait()
     half = trig_ref.shape[1] // 2
     lane = lax.broadcasted_iota(jnp.int32, (1, 2 * half), 1)
     inverse = jnp.zeros((1, 2 * half), jnp.float32)
@@ -114,17 +112,12 @@
         at = 2 * own_rows + s
         trig_ref[at : at + 1, :] = jnp.zeros_like(angles) + lengths_ref[s].astype(jnp.float32)
 
-    copies[3].wait()
-    copies[4].wait()
     hidden = hidden_ref[...]
     normed = norm_rows(hidden, gain_ref[...]).astype(jnp.bfloat16)
     pick_row = lax.broadcasted_iota(jnp.int32, (8, group_rows), 0) + place * own_rows
     pick = jnp.where(pick_row == lax.broadcasted_iota(jnp.int32, (8, group_rows), 1), 1.0, 0.0)
     own = jnp.dot(pick.astype(jnp.bfloat16), hidden, preferred_element_type=jnp.float32)
     own_ref[...] = own[:own_rows].astype(jnp.bfloat16)
-    copies[5].wait()
-    copies[6].wait()
-    copies[7].wait()
     nope = lax.dot_general(
         normed, query_ref[...], NT, preferred_element_type=jnp.float32
     ).astype(jnp.bfloat16)
@@ -199,52 +192,52 @@
             + turned[at] * trig_ref[2 * s + 1 : 2 * s + 2, :]
         ).astype(jnp.bfloat16)
 
-    first = jnp.where(counts[0] <= counts[1], 0, 1)
-
-    @pl.loop(0, rows)
-    def _sequence(i):
-        s = jnp.where(i == 0, first, 1 - first)
-        length = jnp.where(s == 0, lengths[0], lengths[1])
-        blocks = lax.div(length + (BLOCK - 1), BLOCK)
-        for count in range(1, most + 1):
-
-            @pl.when(blocks == count)
-            def _attend(count=count):
-                scores = []
-                for b in range(count):
-                    at = slice(b * BLOCK, (b + 1) * BLOCK)
-                    part = lax.dot_general(
-                        latent_query[s], latent_ref[s, at, :], NT,
-                        preferred_element_type=jnp.float32,
-                    )
-                    part = part + jnp.dot(
-                        rotary_query[s], rope_ref[s, :, at],
-                        preferred_element_type=jnp.float32,
-                    )
-                    part = part * scale
-                    if b == count - 1:
-                        places = b * BLOCK + lax.broadcasted_iota(jnp.int32, (heads, BLOCK), 1)
-                        part = jnp.where(places < length, part, NEG)
-                    scores.append(part)
-                highest = scores[0]
-                for part in scores[1:]:
-                    highest = jnp.maximum(highest, part)
-                highest = jnp.max(highest, axis=1, keepdims=True)
-                weights = [jnp.exp(part - highest) for part in scores]
-                total = weights[0]
-                for part in weights[1:]:
-                    total = total + part
-                factor = 1.0 / jnp.sum(total, axis=1, keepdims=True)
-                summed = None
-                for b in range(count):
-                    probs = (weights[b] * factor).astype(jnp.bfloat16)
-                    at = slice(b * BLOCK, (b + 1) * BLOCK)
-                    term = jnp.dot(
-                        probs, latent_ref[s, at, :],
-                        preferred_element_type=jnp.float32,
-                    )
-                    summed = term if summed is None else summed + term
-                summed_ref[s] = summed.astype(jnp.bfloat16)
+    larger = jnp.where(counts[0] >= counts[1], 0, 1)
+    order = (larger, 1 - larger)
+    ordered = [jnp.where(s == 0, lengths[0], lengths[1]) for s in order]
+    large, small = [lax.div(length + (BLOCK - 1), BLOCK) for length in ordered]
+
+    def score(s, length, b, last):
+        at = slice(b * BLOCK, (b + 1) * BLOCK)
+        part = product(latent_query[s], latent_ref[s, at, :])
+        part = part + jnp.dot(
+            rotary_query[s], rope_ref[s, :, at], preferred_element_type=jnp.float32
+        )
+        part = part * scale
+        if last:
+            places = b * BLOCK + lax.broadcasted_iota(jnp.int32, (heads, BLOCK), 1)
+            part = jnp.where(places < length, part, NEG)
+        return part
+
+    def soften(scores):
+        highest = functools.reduce(jnp.maximum, scores)
+        highest = jnp.max(highest, axis=1, keepdims=True)
+        weights = [jnp.exp(part - highest) for part in scores]
+        total = functools.reduce(jnp.add, weights)
+        factor = 1.0 / jnp.sum(total, axis=1, keepdims=True)
+        return [(part * factor).astype(jnp.bfloat16) for part in weights]
+
+    def weigh(s, probs):
+        terms = [
+            jnp.dot(
+                part, latent_ref[s, b * BLOCK : (b + 1) * BLOCK, :],
+                preferred_element_type=jnp.float32,
+            )
+            for b, part in enumerate(probs)
+        ]
+        summed_ref[s] = functools.reduce(jnp.add, terms).astype(jnp.bfloat16)
+
+    for most_blocks in range(1, most + 1):
+        for least_blocks in range(1, most_blocks + 1):
+
+            @pl.when((large == most_blocks) & (small == least_blocks))
+            def _attend(filled=(most_blocks, least_blocks)):
+                scores = [
+                    [score(s, length, b, b == count - 1) for b in range(count)]
+                    for s, length, count in zip(order, ordered, filled)
+                ]
+                for s, parts in zip(order, scores):
+                    weigh(s, soften(parts))
 
     sums = jnp.concatenate([summed_ref[s] for s in range(rows)], axis=0)
     out_ref[...] = jnp.dot(
@@ -384,7 +377,8 @@
     return lax.dot_general(rows, weight, NT, preferred_element_type=jnp.float32)
 
 
-def enter_kernel(rows_ref, gate_ref, up_ref, gate_out, up_out):
+def enter_kernel(rows_ref, gate_ref, up_ref, down_ref, gate_out, up_out):
+    del down_ref
     rows = rows_ref[...]
     at = half_at(True, rows.shape[1])
     gate_out[...] = product(rows, gate_ref[:, at])
@@ -417,8 +411,8 @@
         enter_kernel,
         "enter",
         (part, part),
-        [VMEM] * 3,
-        (rows, gate_weight, up_weight),
+        [VMEM] * 4,
+        (rows, gate_weight, up_weight, down_weight),
         flops=4 * slots * half * width,
     )
     act, sent = call(

time: 101 us -> 99.8 us (0.988)
  no operation moved by 1% of the time
where the time goes in v4:
time: 99.8 us; the launch traced here: 99.6 us
  blocking collectives  88.6 us (89%)
  Pallas kernels  6.97 us (7%)
  starting transfers between devices  1.71 us (2%)
  waiting for transfers between devices  1.32 us (1%)
    all_to_all x7, blocking collectives, exchanged(): return lax.all_to_all(array, axis, split_axis=0, concat_axis=0, tiled=True)  88.6 us
    pallas_call x9, Pallas kernels, call(): pl.pallas_call(kernel, out_shape=outs, in_specs=ins, out_specs=jax.tree.m...  6.97 us
  transfers between devices with their start and end apart: 2, of which 2 were waited for; matrix products, arithmetic and copies ran while one was open for 0% of the time, Pallas kernels for 1%

profile of v4, /device:TPU:1, one launch (start us, length us, event | category | flops | bytes accessed | tf_op | source)
XLA Modules:
  0.0 99.6 jit_solution(15359066905409644949)
XLA Ops:
  0.0 0.0 copy-start
  0.0 0.0 slice-start
  0.0 0.0 slice-start.1
  0.0 0.0 copy-start.4
  0.0 1.8 %front.1 = (bf16[16,2,544]{2,1,0:T(2,128)(2,1)S(1)}, bf16[2,2048]{1,0:T(2,128)(2,1)S(1)}, f32[2,32]{1,0:T(2,128)S(1)}, f32[32,4]{1,0:T(8,128)S(1)}, f32[6,32]{1,0:T(8,128)S(1)}) custom-call(bf16[32,2048]{1,0:T(8,128)(2,1)} %hidden_hbm.1, f32[1,2048]{1,0:T(1,128)} %bitcast.46, bf16[64,2048]{1,0:T(8,128)(2,1)} %bitcast.43, bf16[32,2048]{1,0:T(8,128)(2,1)} %bitcast.44, ...), custom_call_target="tpu_custom_call" | custom-call | flops 10000000000 | tf_op jit(solution)/shard_map/front/pallas_call | solution.py:24
  1.9 17.4 %all_to_all.35.query_ref = bf16[16,2,544]{2,1,0:T(2,128)(2,1)S(1)} all-to-all(bf16[16,2,544]{2,1,0:T(2,128)(2,1)S(1)} %get-tuple-element.18), channel_id=1, replica_groups=mesh['ep'=16,'tp'=16] {'tp'}, dimensions={0} | all-to-all | bytes 69632 | tf_op jit(solution)/shard_map/all_to_all | solution.py:439
  19.3 0.0 slice-done
  19.3 0.0 slice-done.1
  19.3 0.0 copy-done.4
  19.3 0.0 copy-start.8
  19.4 0.0 copy-start.5
  19.4 0.0 copy-start.6
  19.4 1.5 %attend.1 = bf16[32,512]{1,0:T(8,128)(2,1)S(1)} custom-call(bf16[16,2,544]{2,1,0:T(2,128)(2,1)S(1)} %all_to_all.35.query_ref, f32[6,32]{1,0:T(8,128)S(1)} %get-tuple-element.19.trig_ref, bf16[2,4096,512]{2,1,0:T(8,128)(2,1)S(1)} %bitcast.31, bf16[2,32,4096]{2,1,0:T(8,128)(2,1)S(1)} %copy-done.4), custom_call_target="tpu_custom_call" | custom-call | flops 268435456 | tf_op jit(solution)/shard_map/attend/pallas_call | solution.py:24
  20.9 10.7 %all_to_all.36 = bf16[16,2,512]{2,1,0:T(2,128)(2,1)S(1)} all-to-all(bf16[16,2,512]{2,1,0:T(2,128)(2,1)S(1)} %reshape.33), channel_id=1, replica_groups=mesh['ep'=16,'tp'=16] {'tp'}, dimensions={0} | all-to-all | bytes 65536 | tf_op jit(solution)/shard_map/all_to_all | solution.py:439
  31.6 0.0 copy-done
  31.6 0.0 copy-done.8
  31.6 0.3 convolution_convert_fusion
  31.9 0.1 reshape.35
  32.1 12.0 %all_to_all.37 = bf16[16,2,2048]{2,1,0:T(2,128)(2,1)S(1)} all-to-all(bf16[16,2,2048]{2,1,0:T(2,128)(2,1)S(1)} %reshape.35), channel_id=1, replica_groups=mesh['ep'=16,'tp'=16] {'tp'}, dimensions={0} | all-to-all | bytes 262144 | tf_op jit(solution)/shard_map/all_to_all | solution.py:439
  44.0 0.1 reshape.36.terms_ref
  44.1 0.0 copy-done.5
  44.1 0.0 copy-done.6
  44.1 0.4 mix.1
  44.5 10.2 %all_to_all.38 = bf16[16,2,1024]{2,1,0:T(2,128)(2,1)S(1)} all-to-all(bf16[16,2,1024]{2,1,0:T(2,128)(2,1)S(1)} %get-tuple-element.21), channel_id=1, replica_groups=mesh['ep'=16,'tp'=16] {'tp'}, dimensions={0} | all-to-all | bytes 131072 | tf_op jit(solution)/shard_map/all_to_all | solution.py:439
  54.7 0.0 copy-start.1
  54.7 0.0 copy-start.2
  54.7 0.0 copy-start.3
  54.7 0.2 dispatch.1
  54.9 15.8 %all_to_all.39 = bf16[16,8,1024]{2,1,0:T(8,128)(2,1)S(1)} all-to-all(bf16[16,8,1024]{2,1,0:T(8,128)(2,1)S(1)} %bitcast.39), channel_id=1, replica_groups=mesh['ep'=16,'tp'=16] {'ep'}, dimensions={0} | all-to-all | bytes 524288 | tf_op jit(solution)/shard_map/all_to_all | solution.py:439
  70.8 1.3 %collective-permute-start = (bf16[128,1024]{1,0:T(8,128)(2,1)S(1)}, bf16[128,1024]{1,0:T(8,128)(2,1)S(1)}, u32[]{:S(2)}, u32[]{:S(2)}) collective-permute-start(bf16[128,1024]{1,0:T(8,128)(2,1)S(1)} %bitcast.36), channel_id=1, source_target_pairs={{0,1},{1,0},{2,3},{3,2},{4,5},{5,4},{6,7},{7,6},{8,9},{9,8},{10,11... | collective-permute-start | bytes 786440 | tf_op jit(solution)/shard_map/ppermute | solution.py:409
  72.1 0.0 copy-done.1
  72.1 0.0 copy-done.2
  72.1 0.0 copy-done.3
  72.1 0.7 enter.1
  72.8 0.5 collective-permute-done.rows_ref
  73.2 0.9 leave.1
  74.2 0.5 collective-permute-start.1
  74.6 0.0 copy-start.7
  74.6 0.3 close.1
  74.9 0.9 collective-permute-done.1
  75.8 0.1 fusion
  75.9 10.8 %all_to_all.40 = bf16[16,8,1024]{2,1,0:T(8,128)(2,1)S(1)} all-to-all(bf16[16,8,1024]{2,1,0:T(8,128)(2,1)S(1)} %fusion), channel_id=1, replica_groups=mesh['ep'=16,'tp'=16] {'ep'}, dimensions={0} | all-to-all | bytes 524288 | tf_op jit(solution)/shard_map/all_to_all | solution.py:439
  86.6 0.3 combine.1
  86.9 11.7 %all_to_all.41 = bf16[16,2,1024]{2,1,0:T(2,128)(2,1)S(1)} all-to-all(bf16[16,2,1024]{2,1,0:T(2,128)(2,1)S(1)} %reshape.42), channel_id=1, replica_groups=mesh['ep'=16,'tp'=16] {'tp'}, dimensions={0} | all-to-all | bytes 131072 | tf_op jit(solution)/shard_map/all_to_all | solution.py:439
  98.7 0.0 copy-done.7
  98.7 0.9 finish.1
  (6 shorter events, 0.1 us)
Async XLA Ops:
  0.0 31.6 %copy-start = (bf16[64,2048]{1,0:T(8,128)(2,1)S(1)}, bf16[64,2048]{1,0:T(8,128)(2,1)}, u32[]{:S(2)}) copy-start(bf16[64,2048]{1,0:T(8,128)(2,1)} %param.27) | copy-start | bytes 786436
  0.0 19.3 %slice-start = ((s8[8388608]{0:T(1024)(128)(4,1)}), s8[4194304]{0:T(1024)(128)(4,1)S(1)}, s32[]{:S(2)}) async-start(s8[8388608]{0:T(1024)(128)(4,1)} %bitcast.30), calls=%async_computation.7 | async-start | bytes 8388608
  0.0 19.3 %slice-start.1 = ((s8[8388608]{0:T(1024)(128)(4,1)}), s8[4194304]{0:T(1024)(128)(4,1)S(1)}, s32[]{:S(2)}) async-start(s8[8388608]{0:T(1024)(128)(4,1)} %bitcast.30), calls=%async_computation.8 | async-start | bytes 8388608
  0.0 19.3 %copy-start.4 = (bf16[2,32,4096]{2,1,0:T(8,128)(2,1)S(1)}, bf16[2,32,4096]{2,1,0:T(8,128)(2,1)}, u32[]{:S(2)}) copy-start(bf16[2,32,4096]{2,1,0:T(8,128)(2,1)} %rope_ref.1) | copy-start | bytes 1572868
  19.3 12.3 %copy-start.8 = (bf16[1,512,64]{1,2,0:T(8,128)(2,1)S(1)}, bf16[1,512,64]{1,2,0:T(8,128)(2,1)}, u32[]{:S(2)}) copy-start(bf16[1,512,64]{1,2,0:T(8,128)(2,1)} %param.26) | copy-start | bytes 196612
  19.4 24.7 %copy-start.5 = (f32[2048]{0:T(1024)S(1)}, f32[2048]{0:T(1024)}, u32[]{:S(2)}) copy-start(f32[2048]{0:T(1024)} %param.28) | copy-start | bytes 24580
  19.4 24.7 %copy-start.6 = (f32[2048]{0:T(1024)S(1)}, f32[2048]{0:T(1024)}, u32[]{:S(2)}) copy-start(f32[2048]{0:T(1024)} %param.29) | copy-start | bytes 24580
  54.7 17.4 %copy-start.1 = (bf16[1,448,2048]{2,1,0:T(8,128)(2,1)S(1)}, bf16[1,448,2048]{2,1,0:T(8,128)(2,1)}, u32[]{:S(2)}) copy-start(bf16[1,448,2048]{2,1,0:T(8,128)(2,1)} %param.34) | copy-start | bytes 5505028
  54.7 17.3 %copy-start.2 = (bf16[1,2048,448]{1,2,0:T(8,128)(2,1)S(1)}, bf16[1,2048,448]{1,2,0:T(8,128)(2,1)}, u32[]{:S(2)}) copy-start(bf16[1,2048,448]{1,2,0:T(8,128)(2,1)} %param.32) | copy-start | bytes 5505028
  54.7 17.3 %copy-start.3 = (bf16[1,2048,448]{1,2,0:T(8,128)(2,1)S(1)}, bf16[1,2048,448]{1,2,0:T(8,128)(2,1)}, u32[]{:S(2)}) copy-start(bf16[1,2048,448]{1,2,0:T(8,128)(2,1)} %param.33) | copy-start | bytes 5505028
  70.8 2.4 %collective-permute-start = (bf16[128,1024]{1,0:T(8,128)(2,1)S(1)}, bf16[128,1024]{1,0:T(8,128)(2,1)S(1)}, u32[]{:S(2)}, u32[]{:S(2)}) collective-permute-start(bf16[128,1024]{1,0:T(8,128)(2,1)S(1)} %bitcast.36), channel_id=1, source_target_pairs={{0,1},{1,0},{2,3},{3,2},{4,5},{5,4},{6,7},{7,6},{8,9},{9,8},{10,11... | collective-permute-start | bytes 786440 | tf_op jit(solution)/shard_map/ppermute | solution.py:409
  74.2 1.6 %collective-permute-start.1 = (bf16[128,1024]{1,0:T(8,128)(2,1)S(1)}, bf16[128,1024]{1,0:T(8,128)(2,1)S(1)}, u32[]{:S(2)}, u32[]{:S(2)}) collective-permute-start(bf16[128,1024]{1,0:T(8,128)(2,1)S(1)} %get-tuple-element.25), channel_id=1, source_target_pairs={{0,1},{1,0},{2,3},{3,2},{4,5},{5,4},{6,7},{7,6},{8,9},{9,8},{10,11... | collective-permute-start | bytes 786440 | tf_op jit(solution)/shard_map/ppermute | solution.py:426
  74.6 24.1 %copy-start.7 = (f32[2048]{0:T(1024)S(1)}, f32[2048]{0:T(1024)}, u32[]{:S(2)}) copy-start(f32[2048]{0:T(1024)} %param.35) | copy-start | bytes 24580

commit v5 on v4

--- a/solution.py
+++ b/solution.py
@@ -171,9 +171,6 @@
     ]
     counts = [lax.div(length + (BLOCK - 1), BLOCK) for length in lengths]
 
-    place = lax.broadcasted_iota(jnp.int32, (rows * heads, rows * heads), 0)
-    other = lax.broadcasted_iota(jnp.int32, (rows * heads, rows * heads), 1)
-    by_head = jnp.where(lax.rem(place, rows) * heads + lax.div(place, rows) == other, 1.0, 0.0)
     swap = lax.broadcasted_iota(jnp.int32, (rope, rope), 0) == lax.rem(
         lax.broadcasted_iota(jnp.int32, (rope, rope), 1) + rope // 2, rope
     )
@@ -225,7 +222,7 @@
             )
             for b, part in enumerate(probs)
         ]
-        summed_ref[s] = functools.reduce(jnp.add, terms).astype(jnp.bfloat16)
+        summed_ref[s] = functools.reduce(jnp.add, terms)
 
     for most_blocks in range(1, most + 1):
         for least_blocks in range(1, most_blocks + 1):
@@ -239,10 +236,11 @@
                 for s, parts in zip(order, scores):
                     weigh(s, soften(parts))
 
-    sums = jnp.concatenate([summed_ref[s] for s in range(rows)], axis=0)
-    out_ref[...] = jnp.dot(
-        by_head.astype(jnp.bfloat16), sums, preferred_element_type=jnp.float32
-    ).astype(jnp.bfloat16)
+    sums = [summed_ref[s] for s in range(rows)]
+    for h in range(heads):
+        out_ref[h] = jnp.concatenate([part[h : h + 1, :] for part in sums], axis=0).astype(
+            jnp.bfloat16
+        )
 
 
 def attend(query, trig, latent, rotary, scale):
@@ -251,13 +249,13 @@
     return call(
         functools.partial(attend_kernel, scale),
         "attend",
-        shape((heads * rows, width), jnp.bfloat16),
+        shape((heads, rows, width), jnp.bfloat16),
         [VMEM] * 4,
         (query, trig, latent, rotary),
         scratch=(
             pltpu.VMEM((rows, heads, width), jnp.bfloat16),
             pltpu.VMEM((rows, heads, rope), jnp.bfloat16),
-            pltpu.VMEM((rows, heads, width), jnp.bfloat16),
+            pltpu.VMEM((rows, heads, width), jnp.float32),
         ),
         limit=ATTEND_LIMIT,
         flops=4 * latent.size * heads,
@@ -324,12 +322,14 @@
     gates = jnp.where(place == columns_ref[:, 0:1], columns_ref[:, 2:3], 0.0)
     gates = gates + jnp.where(place == columns_ref[:, 1:2], columns_ref[:, 3:4], 0.0)
     returned = returned_ref[...]
-    total = None
+    parts = []
     for _ in range(3):
-        part = gates.astype(jnp.bfloat16)
-        term = jnp.dot(part, returned, preferred_element_type=jnp.float32)
-        total = term if total is None else total + term
-        gates = gates - part.astype(jnp.float32)
+        parts.append(gates.astype(jnp.bfloat16))
+        gates = gates - parts[-1].astype(jnp.float32)
+    terms = jnp.dot(
+        jnp.concatenate(parts, axis=0), returned, preferred_element_type=jnp.float32
+    )
+    total = terms[:rows] + terms[rows : 2 * rows] + terms[2 * rows :]
     out_ref[...] = total.astype(jnp.bfloat16)
 
 
@@ -487,7 +487,7 @@
     out_latent = attend(
         query, trig, cache_latent, cache_rotary, score_scale
     )
-    out_latent = exchanged(out_latent.reshape(peers, own_rows, latent_width), "tp")
+    out_latent = exchanged(out_latent, "tp")
     out_latent = out_latent.reshape(group_rows, latent_width)
     head_out = jnp.dot(out_latent, value_up[0], preferred_element_type=jnp.float32)
     head_terms = jnp.dot(

time: 99.8 us -> 100 us (level)
  no operation moved by 1% of the time
where the time goes in v5:
time: 100 us; the launch traced here: 99.7 us
  blocking collectives  88.9 us (89%)
  Pallas kernels  6.81 us (7%)
  starting transfers between devices  1.72 us (2%)
  waiting for transfers between devices  1.32 us (1%)
    all_to_all x7, blocking collectives, exchanged(): return lax.all_to_all(array, axis, split_axis=0, concat_axis=0, tiled=True)  88.9 us
    pallas_call x9, Pallas kernels, call(): pl.pallas_call(kernel, out_shape=outs, in_specs=ins, out_specs=jax.tree.m...  6.81 us
  transfers between devices with their start and end apart: 2, of which 2 were waited for; matrix products, arithmetic and copies ran while one was open for 0% of the time, Pallas kernels for 1%

profile of v5, /device:TPU:1, one launch (start us, length us, event | category | flops | bytes accessed | tf_op | source)
XLA Modules:
  0.0 99.7 jit_solution(4177328821021656257)
XLA Ops:
  0.0 0.0 copy-start
  0.0 0.0 slice-start
  0.0 0.0 slice-start.1
  0.0 0.0 copy-start.4
  0.0 1.8 %front.1 = (bf16[16,2,544]{2,1,0:T(2,128)(2,1)S(1)}, bf16[2,2048]{1,0:T(2,128)(2,1)S(1)}, f32[2,32]{1,0:T(2,128)S(1)}, f32[32,4]{1,0:T(8,128)S(1)}, f32[6,32]{1,0:T(8,128)S(1)}) custom-call(bf16[32,2048]{1,0:T(8,128)(2,1)} %hidden_hbm.1, f32[1,2048]{1,0:T(1,128)} %bitcast.46, bf16[64,2048]{1,0:T(8,128)(2,1)} %bitcast.43, bf16[32,2048]{1,0:T(8,128)(2,1)} %bitcast.44, ...), custom_call_target="tpu_custom_call" | custom-call | flops 10000000000 | tf_op jit(solution)/shard_map/front/pallas_call | solution.py:24
  1.9 17.4 %all_to_all.35.query_ref = bf16[16,2,544]{2,1,0:T(2,128)(2,1)S(1)} all-to-all(bf16[16,2,544]{2,1,0:T(2,128)(2,1)S(1)} %get-tuple-element.18), channel_id=1, replica_groups=mesh['ep'=16,'tp'=16] {'tp'}, dimensions={0} | all-to-all | bytes 69632 | tf_op jit(solution)/shard_map/all_to_all | solution.py:439
  19.3 0.0 slice-done
  19.3 0.0 slice-done.1
  19.3 0.0 copy-done.4
  19.3 0.0 copy-start.8
  19.4 0.0 copy-start.5
  19.4 0.0 copy-start.6
  19.4 1.4 %attend.1 = bf16[16,2,512]{2,1,0:T(2,128)(2,1)S(1)} custom-call(bf16[16,2,544]{2,1,0:T(2,128)(2,1)S(1)} %all_to_all.35.query_ref, f32[6,32]{1,0:T(8,128)S(1)} %get-tuple-element.19.trig_ref, bf16[2,4096,512]{2,1,0:T(8,128)(2,1)S(1)} %bitcast.31, bf16[2,32,4096]{2,1,0:T(8,128)(2,1)S(1)} %copy-done.4), custom_call_target="tpu_custom_call" | custom-call | flops 268435456 | tf_op jit(solution)/shard_map/attend/pallas_call | solution.py:24
  20.8 10.7 %all_to_all.36 = bf16[16,2,512]{2,1,0:T(2,128)(2,1)S(1)} all-to-all(bf16[16,2,512]{2,1,0:T(2,128)(2,1)S(1)} %attend.1), channel_id=1, replica_groups=mesh['ep'=16,'tp'=16] {'tp'}, dimensions={0} | all-to-all | bytes 65536 | tf_op jit(solution)/shard_map/all_to_all | solution.py:439
  31.5 0.0 copy-done
  31.5 0.0 copy-done.8
  31.5 0.3 convolution_convert_fusion
  31.9 0.1 reshape.31
  32.0 12.0 %all_to_all.37 = bf16[16,2,2048]{2,1,0:T(2,128)(2,1)S(1)} all-to-all(bf16[16,2,2048]{2,1,0:T(2,128)(2,1)S(1)} %reshape.31), channel_id=1, replica_groups=mesh['ep'=16,'tp'=16] {'tp'}, dimensions={0} | all-to-all | bytes 262144 | tf_op jit(solution)/shard_map/all_to_all | solution.py:439
  43.9 0.1 reshape.32.terms_ref
  44.0 0.0 copy-done.5
  44.0 0.0 copy-done.6
  44.0 0.4 mix.1
  44.4 10.2 %all_to_all.38 = bf16[16,2,1024]{2,1,0:T(2,128)(2,1)S(1)} all-to-all(bf16[16,2,1024]{2,1,0:T(2,128)(2,1)S(1)} %get-tuple-element.21), channel_id=1, replica_groups=mesh['ep'=16,'tp'=16] {'tp'}, dimensions={0} | all-to-all | bytes 131072 | tf_op jit(solution)/shard_map/all_to_all | solution.py:439
  54.6 0.0 copy-start.1
  54.6 0.0 copy-start.2
  54.6 0.0 copy-start.3
  54.7 0.2 dispatch.1
  54.9 16.2 %all_to_all.39 = bf16[16,8,1024]{2,1,0:T(8,128)(2,1)S(1)} all-to-all(bf16[16,8,1024]{2,1,0:T(8,128)(2,1)S(1)} %bitcast.39), channel_id=1, replica_groups=mesh['ep'=16,'tp'=16] {'ep'}, dimensions={0} | all-to-all | bytes 524288 | tf_op jit(solution)/shard_map/all_to_all | solution.py:439
  71.0 1.3 %collective-permute-start = (bf16[128,1024]{1,0:T(8,128)(2,1)S(1)}, bf16[128,1024]{1,0:T(8,128)(2,1)S(1)}, u32[]{:S(2)}, u32[]{:S(2)}) collective-permute-start(bf16[128,1024]{1,0:T(8,128)(2,1)S(1)} %bitcast.36), channel_id=1, source_target_pairs={{0,1},{1,0},{2,3},{3,2},{4,5},{5,4},{6,7},{7,6},{8,9},{9,8},{10,11... | collective-permute-start | bytes 786440 | tf_op jit(solution)/shard_map/ppermute | solution.py:409
  72.3 0.0 copy-done.1
  72.3 0.0 copy-done.2
  72.3 0.0 copy-done.3
  72.3 0.7 enter.1
  73.0 0.5 collective-permute-done.rows_ref
  73.4 0.9 leave.1
  74.4 0.5 collective-permute-start.1
  74.9 0.0 copy-start.7
  74.9 0.3 close.1
  75.2 0.9 collective-permute-done.1
  76.0 0.1 fusion
  76.1 10.7 %all_to_all.40 = bf16[16,8,1024]{2,1,0:T(8,128)(2,1)S(1)} all-to-all(bf16[16,8,1024]{2,1,0:T(8,128)(2,1)S(1)} %fusion), channel_id=1, replica_groups=mesh['ep'=16,'tp'=16] {'ep'}, dimensions={0} | all-to-all | bytes 524288 | tf_op jit(solution)/shard_map/all_to_all | solution.py:439
  86.8 0.2 combine.1
  87.1 0.1 reshape.38
  87.1 11.7 %all_to_all.41 = bf16[16,2,1024]{2,1,0:T(2,128)(2,1)S(1)} all-to-all(bf16[16,2,1024]{2,1,0:T(2,128)(2,1)S(1)} %reshape.38), channel_id=1, replica_groups=mesh['ep'=16,'tp'=16] {'tp'}, dimensions={0} | all-to-all | bytes 131072 | tf_op jit(solution)/shard_map/all_to_all | solution.py:439
  98.9 0.0 copy-done.7
  98.9 0.8 finish.1
  (4 shorter events, 0.1 us)
Async XLA Ops:
  0.0 31.5 %copy-start = (bf16[64,2048]{1,0:T(8,128)(2,1)S(1)}, bf16[64,2048]{1,0:T(8,128)(2,1)}, u32[]{:S(2)}) copy-start(bf16[64,2048]{1,0:T(8,128)(2,1)} %param.27) | copy-start | bytes 786436
  0.0 19.3 %slice-start = ((s8[8388608]{0:T(1024)(128)(4,1)}), s8[4194304]{0:T(1024)(128)(4,1)S(1)}, s32[]{:S(2)}) async-start(s8[8388608]{0:T(1024)(128)(4,1)} %bitcast.30), calls=%async_computation.7 | async-start | bytes 8388608
  0.0 19.3 %slice-start.1 = ((s8[8388608]{0:T(1024)(128)(4,1)}), s8[4194304]{0:T(1024)(128)(4,1)S(1)}, s32[]{:S(2)}) async-start(s8[8388608]{0:T(1024)(128)(4,1)} %bitcast.30), calls=%async_computation.8 | async-start | bytes 8388608
  0.0 19.3 %copy-start.4 = (bf16[2,32,4096]{2,1,0:T(8,128)(2,1)S(1)}, bf16[2,32,4096]{2,1,0:T(8,128)(2,1)}, u32[]{:S(2)}) copy-start(bf16[2,32,4096]{2,1,0:T(8,128)(2,1)} %rope_ref.1) | copy-start | bytes 1572868
  19.3 12.2 %copy-start.8 = (bf16[1,512,64]{1,2,0:T(8,128)(2,1)S(1)}, bf16[1,512,64]{1,2,0:T(8,128)(2,1)}, u32[]{:S(2)}) copy-start(bf16[1,512,64]{1,2,0:T(8,128)(2,1)} %param.26) | copy-start | bytes 196612
  19.4 24.7 %copy-start.5 = (f32[2048]{0:T(1024)S(1)}, f32[2048]{0:T(1024)}, u32[]{:S(2)}) copy-start(f32[2048]{0:T(1024)} %param.28) | copy-start | bytes 24580
  19.4 24.7 %copy-start.6 = (f32[2048]{0:T(1024)S(1)}, f32[2048]{0:T(1024)}, u32[]{:S(2)}) copy-start(f32[2048]{0:T(1024)} %param.29) | copy-start | bytes 24580
  54.6 17.7 %copy-start.1 = (bf16[1,448,2048]{2,1,0:T(8,128)(2,1)S(1)}, bf16[1,448,2048]{2,1,0:T(8,128)(2,1)}, u32[]{:S(2)}) copy-start(bf16[1,448,2048]{2,1,0:T(8,128)(2,1)} %param.34) | copy-start | bytes 5505028
  54.6 17.7 %copy-start.2 = (bf16[1,2048,448]{1,2,0:T(8,128)(2,1)S(1)}, bf16[1,2048,448]{1,2,0:T(8,128)(2,1)}, u32[]{:S(2)}) copy-start(bf16[1,2048,448]{1,2,0:T(8,128)(2,1)} %param.32) | copy-start | bytes 5505028
  54.6 17.6 %copy-start.3 = (bf16[1,2048,448]{1,2,0:T(8,128)(2,1)S(1)}, bf16[1,2048,448]{1,2,0:T(8,128)(2,1)}, u32[]{:S(2)}) copy-start(bf16[1,2048,448]{1,2,0:T(8,128)(2,1)} %param.33) | copy-start | bytes 5505028
  71.0 2.4 %collective-permute-start = (bf16[128,1024]{1,0:T(8,128)(2,1)S(1)}, bf16[128,1024]{1,0:T(8,128)(2,1)S(1)}, u32[]{:S(2)}, u32[]{:S(2)}) collective-permute-start(bf16[128,1024]{1,0:T(8,128)(2,1)S(1)} %bitcast.36), channel_id=1, source_target_pairs={{0,1},{1,0},{2,3},{3,2},{4,5},{5,4},{6,7},{7,6},{8,9},{9,8},{10,11... | collective-permute-start | bytes 786440 | tf_op jit(solution)/shard_map/ppermute | solution.py:409
  74.4 1.6 %collective-permute-start.1 = (bf16[128,1024]{1,0:T(8,128)(2,1)S(1)}, bf16[128,1024]{1,0:T(8,128)(2,1)S(1)}, u32[]{:S(2)}, u32[]{:S(2)}) collective-permute-start(bf16[128,1024]{1,0:T(8,128)(2,1)S(1)} %get-tuple-element.25), channel_id=1, source_target_pairs={{0,1},{1,0},{2,3},{3,2},{4,5},{5,4},{6,7},{7,6},{8,9},{9,8},{10,11... | collective-permute-start | bytes 786440 | tf_op jit(solution)/shard_map/ppermute | solution.py:426
  74.9 24.0 %copy-start.7 = (f32[2048]{0:T(1024)S(1)}, f32[2048]{0:T(1024)}, u32[]{:S(2)}) copy-start(f32[2048]{0:T(1024)} %param.35) | copy-start | bytes 24580

commit v6 on v5

--- a/solution.py
+++ b/solution.py
@@ -259,6 +259,24 @@
         ),
         limit=ATTEND_LIMIT,
         flops=4 * latent.size * heads,
+    )
+
+
+def heads_kernel(latent_ref, value_ref, out_weight_ref, terms_ref):
+    peers, rows, _ = terms_ref.shape
+    head_out = product(latent_ref[...], value_ref[...]).astype(jnp.bfloat16)
+    terms = jnp.dot(head_out, out_weight_ref[...], preferred_element_type=jnp.float32)
+    for t in range(peers):
+        terms_ref[t] = terms[t * rows : (t + 1) * rows].astype(jnp.bfloat16)
+
+
+def heads_terms(latents, value, out_weight, peers):
+    return call(
+        heads_kernel,
+        "heads",
+        shape((peers, latents.shape[0] // peers, out_weight.shape[1]), jnp.bfloat16),
+        [VMEM] * 3,
+        (latents, value, out_weight),
     )
 
 
@@ -489,11 +507,7 @@
     )
     out_latent = exchanged(out_latent, "tp")
     out_latent = out_latent.reshape(group_rows, latent_width)
-    head_out = jnp.dot(out_latent, value_up[0], preferred_element_type=jnp.float32)
-    head_terms = jnp.dot(
-        head_out.astype(jnp.bfloat16), out_weight, preferred_element_type=jnp.float32
-    )
-    head_terms = head_terms.astype(jnp.bfloat16).reshape(peers, own_rows, features)
+    head_terms = heads_terms(out_latent, value_up[0].T, out_weight, peers)
     head_terms = exchanged(head_terms, "tp").reshape(group_rows, features)
     mixed_rows, normed = mix(head_terms, own_hidden, mixed_gain, moe_gain, peers)
     normed = exchanged(normed, "tp").reshape(group_rows, half)

time: 100 us -> 99.5 us (level)
  blocking collectives: 88.9 us -> 87.7 us
  Pallas kernels: 6.81 us -> 7.87 us
    all_to_all x7, blocking collectives: 88.9 us -> 87.7 us  [exchanged(): return lax.all_to_all(array, axis, split_axis=0, concat_axis=0, tiled=True)]
    pallas_call x9 -> x10, Pallas kernels: 6.81 us -> 7.87 us  [call(): pl.pallas_call(kernel, out_shape=outs, in_specs=ins, out_specs=jax.tree.m...]
where the time goes in v6:
time: 99.5 us; the launch traced here: 99.1 us
  blocking collectives  87.7 us (88%)
  Pallas kernels  7.87 us (8%)
  starting transfers between devices  1.71 us (2%)
  waiting for transfers between devices  1.32 us (1%)
    all_to_all x7, blocking collectives, exchanged(): return lax.all_to_all(array, axis, split_axis=0, concat_axis=0, tiled=True)  87.7 us
    pallas_call x10, Pallas kernels, call(): pl.pallas_call(kernel, out_shape=outs, in_specs=ins, out_specs=jax.tree.m...  7.87 us
  transfers between devices with their start and end apart: 2, of which 2 were waited for; matrix products, arithmetic and copies ran while one was open for 0% of the time, Pallas kernels for 1%

profile of v6, /device:TPU:1, one launch (start us, length us, event | category | flops | bytes accessed | tf_op | source)
XLA Modules:
  0.0 99.1 jit_solution(2456342152715243752)
XLA Ops:
  0.0 0.0 slice-start
  0.0 0.0 slice-start.1
  0.0 0.0 copy-start.3
  0.0 1.8 %front.1 = (bf16[16,2,544]{2,1,0:T(2,128)(2,1)S(1)}, bf16[2,2048]{1,0:T(2,128)(2,1)S(1)}, f32[2,32]{1,0:T(2,128)S(1)}, f32[32,4]{1,0:T(8,128)S(1)}, f32[6,32]{1,0:T(8,128)S(1)}) custom-call(bf16[32,2048]{1,0:T(8,128)(2,1)} %hidden_hbm.1, f32[1,2048]{1,0:T(1,128)} %bitcast.44, bf16[64,2048]{1,0:T(8,128)(2,1)} %bitcast.41, bf16[32,2048]{1,0:T(8,128)(2,1)} %bitcast.42, ...), custom_call_target="tpu_custom_call" | custom-call | flops 10000000000 | tf_op jit(solution)/shard_map/front/pallas_call | solution.py:24
  1.9 17.4 %all_to_all.35.query_ref = bf16[16,2,544]{2,1,0:T(2,128)(2,1)S(1)} all-to-all(bf16[16,2,544]{2,1,0:T(2,128)(2,1)S(1)} %get-tuple-element.18), channel_id=1, replica_groups=mesh['ep'=16,'tp'=16] {'tp'}, dimensions={0} | all-to-all | bytes 69632 | tf_op jit(solution)/shard_map/all_to_all | solution.py:457
  19.3 0.0 slice-done
  19.3 0.0 slice-done.1
  19.3 0.0 copy-done.3
  19.3 0.0 copy-start.4
  19.3 0.0 copy-start.5
  19.3 0.0 copy-start.6
  19.4 0.0 copy-start.7
  19.4 2.1 %attend.1 = bf16[16,2,512]{2,1,0:T(2,128)(2,1)S(1)} custom-call(bf16[16,2,544]{2,1,0:T(2,128)(2,1)S(1)} %all_to_all.35.query_ref, f32[6,32]{1,0:T(8,128)S(1)} %get-tuple-element.19.trig_ref, bf16[2,4096,512]{2,1,0:T(8,128)(2,1)S(1)} %bitcast.28, bf16[2,32,4096]{2,1,0:T(8,128)(2,1)S(1)} %copy-done.3), custom_call_target="tpu_custom_call" | custom-call | flops 268435456 | tf_op jit(solution)/shard_map/attend/pallas_call | solution.py:24
  21.5 9.9 %all_to_all.36 = bf16[16,2,512]{2,1,0:T(2,128)(2,1)S(1)} all-to-all(bf16[16,2,512]{2,1,0:T(2,128)(2,1)S(1)} %attend.1), channel_id=1, replica_groups=mesh['ep'=16,'tp'=16] {'tp'}, dimensions={0} | all-to-all | bytes 65536 | tf_op jit(solution)/shard_map/all_to_all | solution.py:457
  31.4 0.0 copy-done.4
  31.4 0.0 copy-done.5
  31.5 0.3 heads.1
  31.8 12.0 %all_to_all.37 = bf16[16,2,2048]{2,1,0:T(2,128)(2,1)S(1)} all-to-all(bf16[16,2,2048]{2,1,0:T(2,128)(2,1)S(1)} %heads.1), channel_id=1, replica_groups=mesh['ep'=16,'tp'=16] {'tp'}, dimensions={0} | all-to-all | bytes 262144 | tf_op jit(solution)/shard_map/all_to_all | solution.py:457
  43.8 0.1 reshape.28.terms_ref
  43.8 0.0 copy-done.6
  43.8 0.0 copy-done.7
  43.9 0.4 mix.1
  44.2 10.2 %all_to_all.38 = bf16[16,2,1024]{2,1,0:T(2,128)(2,1)S(1)} all-to-all(bf16[16,2,1024]{2,1,0:T(2,128)(2,1)S(1)} %get-tuple-element.21), channel_id=1, replica_groups=mesh['ep'=16,'tp'=16] {'tp'}, dimensions={0} | all-to-all | bytes 131072 | tf_op jit(solution)/shard_map/all_to_all | solution.py:457
  54.4 0.0 copy-start
  54.5 0.0 copy-start.1
  54.5 0.0 copy-start.2
  54.5 0.2 dispatch.1
  54.7 15.7 %all_to_all.39 = bf16[16,8,1024]{2,1,0:T(8,128)(2,1)S(1)} all-to-all(bf16[16,8,1024]{2,1,0:T(8,128)(2,1)S(1)} %bitcast.36), channel_id=1, replica_groups=mesh['ep'=16,'tp'=16] {'ep'}, dimensions={0} | all-to-all | bytes 524288 | tf_op jit(solution)/shard_map/all_to_all | solution.py:457
  70.4 1.3 %collective-permute-start = (bf16[128,1024]{1,0:T(8,128)(2,1)S(1)}, bf16[128,1024]{1,0:T(8,128)(2,1)S(1)}, u32[]{:S(2)}, u32[]{:S(2)}) collective-permute-start(bf16[128,1024]{1,0:T(8,128)(2,1)S(1)} %bitcast.33), channel_id=1, source_target_pairs={{0,1},{1,0},{2,3},{3,2},{4,5},{5,4},{6,7},{7,6},{8,9},{9,8},{10,11... | collective-permute-start | bytes 786440 | tf_op jit(solution)/shard_map/ppermute | solution.py:427
  71.7 0.0 copy-done
  71.7 0.0 copy-done.1
  71.7 0.0 copy-done.2
  71.7 0.7 enter.1
  72.4 0.5 collective-permute-done.rows_ref
  72.8 0.9 leave.1
  73.8 0.5 collective-permute-start.1
  74.2 0.0 copy-start.8
  74.2 0.3 close.1
  74.5 0.9 collective-permute-done.1
  75.4 0.1 fusion
  75.5 10.8 %all_to_all.40 = bf16[16,8,1024]{2,1,0:T(8,128)(2,1)S(1)} all-to-all(bf16[16,8,1024]{2,1,0:T(8,128)(2,1)S(1)} %fusion), channel_id=1, replica_groups=mesh['ep'=16,'tp'=16] {'ep'}, dimensions={0} | all-to-all | bytes 524288 | tf_op jit(solution)/shard_map/all_to_all | solution.py:457
  86.2 0.2 combine.1
  86.4 0.1 reshape.34
  86.5 11.7 %all_to_all.41 = bf16[16,2,1024]{2,1,0:T(2,128)(2,1)S(1)} all-to-all(bf16[16,2,1024]{2,1,0:T(2,128)(2,1)S(1)} %reshape.34), channel_id=1, replica_groups=mesh['ep'=16,'tp'=16] {'tp'}, dimensions={0} | all-to-all | bytes 131072 | tf_op jit(solution)/shard_map/all_to_all | solution.py:457
  98.3 0.0 copy-done.8
  98.3 0.8 finish.1
  (4 shorter events, 0.1 us)
Async XLA Ops:
  0.0 19.3 %slice-start = ((s8[8388608]{0:T(1024)(128)(4,1)}), s8[4194304]{0:T(1024)(128)(4,1)S(1)}, s32[]{:S(2)}) async-start(s8[8388608]{0:T(1024)(128)(4,1)} %bitcast.27), calls=%async_computation.7 | async-start | bytes 8388608
  0.0 19.3 %slice-start.1 = ((s8[8388608]{0:T(1024)(128)(4,1)}), s8[4194304]{0:T(1024)(128)(4,1)S(1)}, s32[]{:S(2)}) async-start(s8[8388608]{0:T(1024)(128)(4,1)} %bitcast.27), calls=%async_computation.8 | async-start | bytes 8388608
  0.0 19.3 %copy-start.3 = (bf16[2,32,4096]{2,1,0:T(8,128)(2,1)S(1)}, bf16[2,32,4096]{2,1,0:T(8,128)(2,1)}, u32[]{:S(2)}) copy-start(bf16[2,32,4096]{2,1,0:T(8,128)(2,1)} %rope_ref.1) | copy-start | bytes 1572868
  19.3 12.1 %copy-start.4 = (bf16[64,2048]{1,0:T(8,128)(2,1)S(1)}, bf16[64,2048]{1,0:T(8,128)(2,1)}, u32[]{:S(2)}) copy-start(bf16[64,2048]{1,0:T(8,128)(2,1)} %out_weight_ref.1) | copy-start | bytes 786436
  19.3 12.1 %copy-start.5 = (bf16[1,512,64]{1,2,0:T(8,128)(2,1)S(1)}, bf16[1,512,64]{1,2,0:T(8,128)(2,1)}, u32[]{:S(2)}) copy-start(bf16[1,512,64]{1,2,0:T(8,128)(2,1)} %param.26) | copy-start | bytes 196612
  19.3 24.5 %copy-start.6 = (f32[2048]{0:T(1024)S(1)}, f32[2048]{0:T(1024)}, u32[]{:S(2)}) copy-start(f32[2048]{0:T(1024)} %param.28) | copy-start | bytes 24580
  19.4 24.5 %copy-start.7 = (f32[2048]{0:T(1024)S(1)}, f32[2048]{0:T(1024)}, u32[]{:S(2)}) copy-start(f32[2048]{0:T(1024)} %param.29) | copy-start | bytes 24580
  54.4 17.2 %copy-start = (bf16[1,448,2048]{2,1,0:T(8,128)(2,1)S(1)}, bf16[1,448,2048]{2,1,0:T(8,128)(2,1)}, u32[]{:S(2)}) copy-start(bf16[1,448,2048]{2,1,0:T(8,128)(2,1)} %param.34) | copy-start | bytes 5505028
  54.5 17.2 %copy-start.1 = (bf16[1,2048,448]{1,2,0:T(8,128)(2,1)S(1)}, bf16[1,2048,448]{1,2,0:T(8,128)(2,1)}, u32[]{:S(2)}) copy-start(bf16[1,2048,448]{1,2,0:T(8,128)(2,1)} %param.32) | copy-start | bytes 5505028
  54.5 17.2 %copy-start.2 = (bf16[1,2048,448]{1,2,0:T(8,128)(2,1)S(1)}, bf16[1,2048,448]{1,2,0:T(8,128)(2,1)}, u32[]{:S(2)}) copy-start(bf16[1,2048,448]{1,2,0:T(8,128)(2,1)} %param.33) | copy-start | bytes 5505028
  70.4 2.4 %collective-permute-start = (bf16[128,1024]{1,0:T(8,128)(2,1)S(1)}, bf16[128,1024]{1,0:T(8,128)(2,1)S(1)}, u32[]{:S(2)}, u32[]{:S(2)}) collective-permute-start(bf16[128,1024]{1,0:T(8,128)(2,1)S(1)} %bitcast.33), channel_id=1, source_target_pairs={{0,1},{1,0},{2,3},{3,2},{4,5},{5,4},{6,7},{7,6},{8,9},{9,8},{10,11... | collective-permute-start | bytes 786440 | tf_op jit(solution)/shard_map/ppermute | solution.py:427
  73.8 1.6 %collective-permute-start.1 = (bf16[128,1024]{1,0:T(8,128)(2,1)S(1)}, bf16[128,1024]{1,0:T(8,128)(2,1)S(1)}, u32[]{:S(2)}, u32[]{:S(2)}) collective-permute-start(bf16[128,1024]{1,0:T(8,128)(2,1)S(1)} %get-tuple-element.25), channel_id=1, source_target_pairs={{0,1},{1,0},{2,3},{3,2},{4,5},{5,4},{6,7},{7,6},{8,9},{9,8},{10,11... | collective-permute-start | bytes 786440 | tf_op jit(solution)/shard_map/ppermute | solution.py:444
  74.2 24.0 %copy-start.8 = (f32[2048]{0:T(1024)S(1)}, f32[2048]{0:T(1024)}, u32[]{:S(2)}) copy-start(f32[2048]{0:T(1024)} %param.35) | copy-start | bytes 24580
